TPU v7x, 256 devices: a whole 4x4x8 slice. The times are simulated.
256 devices in a mesh: ep: 128 (over z, y, x), tp: 2 (over core).
Axes of the slice: x: 4, y: 4, z: 8, core: 2. Of those that a mesh axis runs over, the one named last changes fastest.
Arguments:
- tokens: bfloat16 [256, 2048], P('ep'), may hold values from -6 to 6
- head_state: float32 [256, 32, 64, 128], P('ep', 'tp'), may hold values from -4 to 4
- conv_state: bfloat16 [256, 3, 2048], P('ep', None, 'tp'), may hold values from -6 to 6
- conv_proj_state: bfloat16 [256, 3, 2, 512], P('ep', None, None, 'tp'), may hold values from -6 to 6
- first_gain: float32 [2048], replicated, may hold values from 0.1 to 1.9
- gate_weight: bfloat16 [2048, 2048], P('ep', 'tp'), may hold values from -0.125 to 0.125
- inner_weight: bfloat16 [2048, 2048], P('ep', 'tp'), may hold values from -0.125 to 0.125
- write_weight: bfloat16 [2048, 512], P(None, 'tp'), may hold values from -0.125 to 0.125
- read_weight: bfloat16 [2048, 512], P(None, 'tp'), may hold values from -0.125 to 0.125
- step_weight: bfloat16 [2048, 32], P(None, 'tp'), may hold values from -0.125 to 0.125
- conv_kernel: float32 [4, 2048], P(None, 'tp'), may hold values from -3 to 3
- conv_proj_kernel: float32 [4, 2, 512], P(None, None, 'tp'), may hold values from -3 to 3
- step_bias: float32 [32], P('tp'), may hold values from -2 to 1
- log_rate: float32 [32], P('tp'), may hold values from -4.5 to 1.5
- skip_gain: float32 [32], P('tp'), may hold values from 0.5 to 2
- group_gain: float32 [2048], P('tp'), may hold values from 0.1 to 1.9
- out_weight: bfloat16 [2048, 2048], P('tp', 'ep'), may hold values from -0.125 to 0.125
- second_gain: float32 [2048], replicated, may hold values from 0.1 to 1.9
- routes: int32 [256, 4], P('ep'), may hold values from 0 to 127, all different within a row; in each aligned block of 256 rows (0 to 255, 256 to 511, ...) at most 32 rows name the same one
- route_logits: bfloat16 [256, 4], P('ep'), may hold values from -8 to 300
- expert_gate: bfloat16 [128, 2048, 1024], P('ep', None, 'tp'), may hold values from -0.5 to 0.5
- expert_up: bfloat16 [128, 2048, 1024], P('ep', None, 'tp'), may hold values from -0.5 to 0.5
- expert_down: bfloat16 [128, 1024, 2048], P('ep', 'tp'), may hold values from -0.0234375 to 0.0234375
- dense_up: bfloat16 [2048, 4096], P(None, ('ep', 'tp')), may hold values from -0.125 to 0.125
- dense_down: bfloat16 [4096, 2048], P(('ep', 'tp')), may hold values from -0.09375 to 0.09375
- dense_gate: float32 [2048], replicated, may hold values from -0.125 to 0.125
Outputs:
- layer_out: bfloat16 [256, 2048], P(('ep', 'tp'))
- state_out: float32 [256, 32, 64, 128], P('ep', 'tp')
- conv_out: bfloat16 [256, 3, 2048], P('ep', None, 'tp')
- conv_proj_out: bfloat16 [256, 3, 2, 512], P('ep', None, None, 'tp')
Inputs may be any that keep to these rules, and one draw needn't show every extreme that they name: `routes`: each token names 4 different experts; over the whole batch no expert is named by more than 32 rows, a bound that some block reaches.
All inputs are finite; a program needn't handle non-finite values.
Results may differ from a plain program's by a relative error of at most 0.015.
Values may be sent and summed in bfloat16 or wider, within the bound.
A program may use at most 64 MiB of HBM per device.

v0:
```python
import jax
import jax.numpy as jnp
from jax import lax
from jax.sharding import Mesh
from jax.sharding import PartitionSpec as P

GROUPS = 4
EP = ("ep_0", "ep_1", "ep_2")
EP_TP = ("ep_0", "ep_1", "ep_2", "tp")


norm_eps = 1e-05
clamp_limit = 7.0
glu_alpha = 1.702
highest = lax.Precision.HIGHEST


def in_one_piece(arrays, axis, dim, along):
    widths = [a.shape[along] for a in arrays]
    both = jnp.concatenate(arrays, axis=along)
    result = lax.all_gather(both, axis, axis=dim, tiled=True)
    return tuple(jnp.split(result, [sum(widths[:k]) for k in range(1, len(widths))], axis=along))


def gathered_by_axis(shard, axes, dim):
    if not axes:
        return shard
    nearer = lax.all_gather(shard, axes[-1], axis=dim, tiled=True)
    return gathered_by_axis(nearer, axes[:-1], dim)


def sent_to_all(shard, axis):
    copies = jnp.broadcast_to(shard, (lax.axis_size(axis), *shard.shape))
    return lax.all_to_all(copies, axis, split_axis=0, concat_axis=0, tiled=True)


def over_copies(shard, axis):
    everything = sent_to_all(shard, axis)
    return jnp.sum(everything, axis=0)


def rms_scale(values, gain_vec):
    return (
        values * lax.rsqrt(jnp.mean(values * values, axis=-1, keepdims=True) + norm_eps) * gain_vec
    )


def clamped_unit(gate_pre, up_pre):
    glu_part = jnp.minimum(gate_pre, clamp_limit)
    lin_part = jnp.clip(up_pre, -clamp_limit, clamp_limit)
    return glu_part * jax.nn.sigmoid(glu_alpha * glu_part) * (lin_part + 1.0)


def state_step(
    inner_proj,
    gate_proj,
    write_proj,
    read_proj,
    step_raw,
    conv_state,
    conv_proj_state,
    conv_kernel,
    conv_proj_kernel,
    step_bias,
    log_rate,
    skip_gain,
    group_gain,
    head_state,
    group_count,
):
    window_inner = jnp.concatenate([conv_state, inner_proj[:, None, :]], axis=1)
    window_proj = jnp.concatenate(
        [conv_proj_state, jnp.stack([write_proj, read_proj], axis=1)[:, None]], axis=1
    )
    conv_inner = jax.nn.silu(jnp.sum(window_inner.astype(jnp.float32) * conv_kernel[None], axis=1))
    conv_proj = jax.nn.silu(
        jnp.sum(window_proj.astype(jnp.float32) * conv_proj_kernel[None], axis=1)
    )
    seq_count, channels = conv_inner.shape
    head_count = step_raw.shape[1]
    head_width = channels // head_count
    state_width = conv_proj.shape[2] // group_count
    per_group = head_count // group_count
    head_input = conv_inner.reshape(seq_count, head_count, head_width)
    write_heads = jnp.repeat(
        conv_proj[:, 0].reshape(seq_count, group_count, state_width), per_group, axis=1
    )
    read_heads = jnp.repeat(
        conv_proj[:, 1].reshape(seq_count, group_count, state_width), per_group, axis=1
    )
    step_size = jax.nn.softplus(step_raw + step_bias)
    decay_rate = jnp.exp(-jnp.exp(log_rate) * step_size)
    state_out = (
        decay_rate[:, :, None, None] * head_state
        + (step_size[:, :, None] * head_input)[:, :, :, None] * write_heads[:, :, None, :]
    )
    read_out = (
        jnp.einsum("shpn,shn->shp", state_out, read_heads, precision=highest)
        + skip_gain[None, :, None] * head_input
    )
    gated_rows = read_out.reshape(seq_count, channels) * jax.nn.silu(gate_proj.astype(jnp.float32))
    grouped = gated_rows.reshape(seq_count, group_count, channels // group_count)
    grouped = grouped * lax.rsqrt(jnp.mean(grouped * grouped, axis=-1, keepdims=True) + norm_eps)
    mixer_rows = (grouped.reshape(seq_count, channels) * group_gain).astype(jnp.bfloat16)
    return (mixer_rows, state_out, window_inner[:, 1:], window_proj[:, 1:])


def local(
    tokens,
    head_state,
    conv_state,
    conv_proj_state,
    first_gain,
    gate_weight,
    inner_weight,
    write_weight,
    read_weight,
    step_weight,
    conv_kernel,
    conv_proj_kernel,
    step_bias,
    log_rate,
    skip_gain,
    group_gain,
    out_weight,
    second_gain,
    routes,
    route_logits,
    expert_gate,
    expert_up,
    expert_down,
    dense_up,
    dense_down,
    dense_gate,
):
    seq_count = tokens.shape[0]
    normed_in = rms_scale(tokens.astype(jnp.float32), first_gain).astype(jnp.bfloat16)
    pieces = in_one_piece((gate_weight, inner_weight), EP, 0, 1)
    gate_sum = jnp.dot(normed_in, pieces[0], preferred_element_type=jnp.float32)
    inner_sum = jnp.dot(normed_in, pieces[1], preferred_element_type=jnp.float32)
    gate_proj = gate_sum.astype(jnp.bfloat16)
    inner_proj = inner_sum.astype(jnp.bfloat16)
    write_proj = jnp.dot(normed_in, write_weight, preferred_element_type=jnp.float32).astype(
        jnp.bfloat16
    )
    read_proj = jnp.dot(normed_in, read_weight, preferred_element_type=jnp.float32).astype(
        jnp.bfloat16
    )
    step_raw = jnp.dot(normed_in, step_weight, preferred_element_type=jnp.float32)
    local_groups = GROUPS // lax.axis_size("tp")
    mixer_rows, state_out, conv_out, conv_proj_out = state_step(
        inner_proj,
        gate_proj,
        write_proj,
        read_proj,
        step_raw,
        conv_state,
        conv_proj_state,
        conv_kernel,
        conv_proj_kernel,
        step_bias,
        log_rate,
        skip_gain,
        group_gain,
        head_state,
        local_groups,
    )
    column_block = jnp.dot(
        gathered_by_axis(mixer_rows, EP, 0), out_weight, preferred_element_type=jnp.float32
    )
    partial_mix = lax.all_to_all(column_block, EP, split_axis=0, concat_axis=1, tiled=True)
    mixed = over_copies(partial_mix, "tp")
    hidden = (tokens.astype(jnp.float32) + mixed).astype(jnp.bfloat16)
    normed_mid = rms_scale(hidden.astype(jnp.float32), second_gain).astype(jnp.bfloat16)
    all_rows, all_routes, all_logits = (
        gathered_by_axis(normed_mid, EP, 0),
        gathered_by_axis(routes, EP, 0),
        gathered_by_axis(route_logits, EP, 0),
    )
    route_gates = jax.nn.softmax(all_logits.astype(jnp.float32), axis=-1)
    my_expert = lax.axis_index(EP)
    route_hits = all_routes == my_expert
    row_weight = jnp.sum(jnp.where(route_hits, route_gates, 0.0), axis=1)
    chosen = jnp.any(route_hits, axis=1)
    slot_index = jnp.cumsum(chosen.astype(jnp.int32)) - 1
    capacity = 4 * seq_count * routes.shape[1]
    slot_ids = jnp.arange(capacity, dtype=jnp.int32)
    picks = (slot_index[None, :] == slot_ids[:, None]) & chosen[None, :]
    picked_rows = jnp.dot(
        picks.astype(jnp.bfloat16), all_rows, preferred_element_type=jnp.float32
    ).astype(jnp.bfloat16)
    activated = clamped_unit(
        jnp.dot(picked_rows, expert_gate[0], preferred_element_type=jnp.float32),
        jnp.dot(picked_rows, expert_up[0], preferred_element_type=jnp.float32),
    ).astype(jnp.bfloat16)
    expert_part = jnp.dot(activated, expert_down[0], preferred_element_type=jnp.float32)
    placed = jnp.where(picks, row_weight[None, :], 0.0)
    dense_weight = jax.nn.sigmoid(
        jnp.dot(all_rows.astype(jnp.float32), dense_gate, precision=highest)
    )
    row_share = seq_count // lax.axis_size("tp")
    down_half = lax.all_to_all(dense_down, "tp", split_axis=1, concat_axis=0, tiled=True)
    dense_inner = jax.nn.silu(
        jnp.dot(all_rows, dense_up, preferred_element_type=jnp.float32)
    ).astype(jnp.bfloat16)
    pair_inner = lax.all_gather(dense_inner, "tp", axis=1, tiled=True)
    expert_cols = lax.psum_scatter(
        expert_part.astype(jnp.bfloat16), "tp", scatter_dimension=1, tiled=True
    ).astype(jnp.float32)
    dense_term = (
        jnp.dot(pair_inner, down_half, preferred_element_type=jnp.float32) * dense_weight[:, None]
    )
    column_sums = lax.psum_scatter(
        dense_term + jnp.einsum("cr,cd->rd", placed, expert_cols, precision=highest),
        EP,
        scatter_dimension=0,
        tiled=True,
    )
    summed = lax.all_to_all(column_sums, "tp", split_axis=0, concat_axis=1, tiled=True)
    own_rows = lax.dynamic_slice_in_dim(hidden, lax.axis_index("tp") * row_share, row_share, 0)
    layer_out = (own_rows.astype(jnp.float32) + summed).astype(jnp.bfloat16)
    return (layer_out, state_out, conv_out, conv_proj_out)


def solution(mesh):
    torus = Mesh(mesh.devices.reshape(8, 4, 4, mesh.shape["tp"]), ("ep_0", "ep_1", "ep_2", "tp"))
    return jax.shard_map(
        local,
        mesh=torus,
        in_specs=(
            P(EP, None),
            P(EP, "tp", None, None),
            P(EP, None, "tp"),
            P(EP, None, None, "tp"),
            P(),
            P(EP, "tp"),
            P(EP, "tp"),
            P(None, "tp"),
            P(None, "tp"),
            P(None, "tp"),
            P(None, "tp"),
            P(None, None, "tp"),
            P("tp"),
            P("tp"),
            P("tp"),
            P("tp"),
            P("tp", EP),
            P(),
            P(EP, None),
            P(EP, None),
            P(EP, None, "tp"),
            P(EP, None, "tp"),
            P(EP, "tp", None),
            P(None, EP_TP),
            P(EP_TP, None),
            P(),
        ),
        out_specs=(
            P(EP_TP, None),
            P(EP, "tp", None, None),
            P(EP, None, "tp"),
            P(EP, None, None, "tp"),
        ),
        check_vma=False,
    )
```

profile of v0, /device:TPU:1, one launch (start us, length us, event | category | flops | bytes accessed | tf_op | source)
XLA Modules:
  0.0 581.7 jit_solution(3944706384839282891)
XLA Ops:
  13.3 123.4 %all-gather.11.cloned.1.call-done = bf16[2048,2048]{1,0:T(8,128)(2,1)} async-done(((bf16[16,2048]{1,0:T(8,128)(2,1)}), bf16[2048,2048]{1,0:T(8,128)(2,1)}) %all-gather.11.cloned.1.call-update) | async-done | bytes 8388624 | tf_op jit(solution)/shard_map/all_gather | solution.py:21
  136.7 2.9 fusion.35
  143.0 2.9 fusion.88
  146.2 9.4 %all-gather = bf16[4,2,1024]{2,1,0:T(2,128)(2,1)S(1)} all-gather(bf16[1,2,1024]{2,1,0:T(2,128)(2,1)S(1)} %fusion.72), channel_id=1, replica_groups=mesh['ep_0'=8,'ep_1'=4,'ep_2'=4,'tp'=2] {'ep_2'}, dimensions={0}, use_global_device_ids=true | all-gather | bytes 20480 | tf_op jit(solution)/shard_map/all_gather | solution.py:28
  155.7 9.0 %all_gather.44 = bf16[32,1024]{1,0:T(8,128)(2,1)S(1)} all-gather(bf16[8,1024]{1,0:T(8,128)(2,1)S(1)} %reshape.119), channel_id=1, replica_groups=mesh['ep_0'=8,'ep_1'=4,'ep_2'=4,'tp'=2] {'ep_1'}, dimensions={0}, use_global_device_ids=true | all-gather | bytes 81920 | tf_op jit(solution)/shard_map/all_gather | solution.py:28
  164.7 20.8 %all_gather.45 = bf16[256,1024]{1,0:T(8,128)(2,1)S(1)} all-gather(bf16[32,1024]{1,0:T(8,128)(2,1)S(1)} %all_gather.44), channel_id=1, replica_groups=mesh['ep_0'=8,'ep_1'=4,'ep_2'=4,'tp'=2] {'ep_0'}, dimensions={0}, use_global_device_ids=true | all-gather | bytes 589824 | tf_op jit(solution)/shard_map/all_gather | solution.py:28
  185.7 19.8 %all_to_all.59 = f32[128,2,16]{2,1,0:T(2,128)S(1)} all-to-all(f32[128,2,16]{2,1,0:T(2,128)S(1)} %bitcast.96), channel_id=1, replica_groups=mesh['ep_0'=8,'ep_1'=4,'ep_2'=4,'tp'=2] {'ep_0','ep_1','ep_2'}, dimensions={0} | all-to-all | bytes 32768 | tf_op jit(solution)/shard_map/all_to_all | solution.py:171
  205.6 20.4 %all_to_all.60 = f32[2,2,2048]{2,1,0:T(2,128)S(1)} all-to-all(f32[2,2,2048]{2,1,0:T(2,128)S(1)} %broadcast_in_dim.26), channel_id=1, replica_groups=mesh['ep_0'=8,'ep_1'=4,'ep_2'=4,'tp'=2] {'tp'}, dimensions={0} | all-to-all | bytes 65536 | tf_op jit(solution)/shard_map/all_to_all | solution.py:34
  226.3 9.0 %all-gather.1 = bf16[4,2,2048]{2,1,0:T(2,128)(2,1)S(1)} all-gather(bf16[1,2,2048]{2,1,0:T(2,128)(2,1)S(1)} %fusion.71), channel_id=1, replica_groups=mesh['ep_0'=8,'ep_1'=4,'ep_2'=4,'tp'=2] {'ep_2'}, dimensions={0}, use_global_device_ids=true | all-gather | bytes 40960 | tf_op jit(solution)/shard_map/all_gather | solution.py:28
  235.3 10.3 %all_gather.47 = bf16[32,2048]{1,0:T(8,128)(2,1)} all-gather(bf16[8,2048]{1,0:T(8,128)(2,1)S(1)} %reshape.121), channel_id=1, replica_groups=mesh['ep_0'=8,'ep_1'=4,'ep_2'=4,'tp'=2] {'ep_1'}, dimensions={0}, use_global_device_ids=true | all-gather | bytes 163840 | tf_op jit(solution)/shard_map/all_gather | solution.py:28
  246.3 8.9 %all-to-all-start.2 = ((bf16[16,2,1024]{2,0,1:T(8,128)(2,1)}), bf16[16,2,1024]{2,0,1:T(8,128)(2,1)S(1)}, u32[]{:S(2)}, u32[]{:S(2)}) async-start(bf16[16,2,1024]{2,0,1:T(8,128)(2,1)} %bitcast.94), calls=%async_computation.2 | async-start | bytes 131072 | tf_op jit(solution)/shard_map/all_to_all | solution.py:202
  255.2 5.8 %all-gather.5 = bf16[4,2,4]{2,1,0:T(2,128)(2,1)S(1)} all-gather(bf16[1,2,4]{2,1,0:T(2,128)(2,1)S(1)} %bitcast.110), channel_id=1, replica_groups=mesh['ep_0'=8,'ep_1'=4,'ep_2'=4,'tp'=2] {'ep_2'}, dimensions={0}, use_global_device_ids=true | all-gather | bytes 80 | tf_op jit(solution)/shard_map/all_gather | solution.py:28
  261.1 7.1 %all-gather.2 = s32[4,2,4]{2,1,0:T(2,128)S(1)} all-gather(s32[1,2,4]{2,1,0:T(2,128)S(1)} %bitcast.109), channel_id=1, replica_groups=mesh['ep_0'=8,'ep_1'=4,'ep_2'=4,'tp'=2] {'ep_2'}, dimensions={0}, use_global_device_ids=true | all-gather | bytes 160 | tf_op jit(solution)/shard_map/all_gather | solution.py:28
  268.3 8.6 %all-gather.3 = s32[4,8,4]{1,2,0:T(4,128)S(1)} all-gather(s32[1,8,4]{1,2,0:T(4,128)S(1)} %copy.74), channel_id=1, replica_groups=mesh['ep_0'=8,'ep_1'=4,'ep_2'=4,'tp'=2] {'ep_1'}, dimensions={0}, use_global_device_ids=true | all-gather | bytes 640 | tf_op jit(solution)/shard_map/all_gather | solution.py:28
  277.0 16.0 %all-gather.4 = s32[8,32,4]{1,2,0:T(4,128)S(1)} all-gather(s32[1,32,4]{1,2,0:T(4,128)S(1)} %reshape.126), channel_id=1, replica_groups=mesh['ep_0'=8,'ep_1'=4,'ep_2'=4,'tp'=2] {'ep_0'}, dimensions={0}, use_global_device_ids=true | all-gather | bytes 4608 | tf_op jit(solution)/shard_map/all_gather | solution.py:28
  293.7 5.3 all-gather.6
  299.2 9.8 %all-gather.7 = bf16[8,32,4]{1,2,0:T(4,128)(2,1)S(1)} all-gather(bf16[1,32,4]{1,2,0:T(4,128)(2,1)S(1)} %reshape.132), channel_id=1, replica_groups=mesh['ep_0'=8,'ep_1'=4,'ep_2'=4,'tp'=2] {'ep_0'}, dimensions={0}, use_global_device_ids=true | all-gather | bytes 2304 | tf_op jit(solution)/shard_map/all_gather | solution.py:28
  310.9 2.0 fusion.9
  313.0 3.2 convolution_convert_fusion
  317.7 17.9 %all_gather.49 = bf16[256,32]{0,1:T(8,128)(2,1)S(1)} all-gather(bf16[256,16]{0,1:T(8,128)(2,1)S(1)} %multiply_convert_fusion), channel_id=1, replica_groups=mesh['ep_0'=8,'ep_1'=4,'ep_2'=4,'tp'=2] {'tp'}, dimensions={1}, use_global_device_ids=true | all-gather | bytes 24576 | tf_op jit(solution)/shard_map/all_gather | solution.py:206
  336.0 4.8 reduce-scatter.2.cloned.1.call-done
  340.8 2.5 convolution_add_fusion
  345.7 219.4 %all-reduce.3.cloned.1.call-done = f32[256,1024]{1,0:T(8,128)} async-done(((f32[256,1024]{1,0:T(8,128)}), f32[256,1024]{1,0:T(8,128)}) %all-reduce.3.cloned.1.call-update) | async-done | bytes 1048592
  565.9 8.7 %all_to_all.61 = f32[2,1,1024]{2,1,0:T(1,128)S(1)} all-to-all(f32[2,1,1024]{2,1,0:T(1,128)S(1)} %copy.80), channel_id=1, replica_groups=mesh['ep_0'=8,'ep_1'=4,'ep_2'=4,'tp'=2] {'tp'}, dimensions={0} | all-to-all | bytes 16384 | tf_op jit(solution)/shard_map/all_to_all | solution.py:219
  (128 shorter events, 18.8 us)
Async XLA Ops:
  7.2 305.8 %copy-start = (bf16[1,512,2048]{2,1,0:T(8,128)(2,1)S(1)}, bf16[1,512,2048]{2,1,0:T(8,128)(2,1)}, u32[]{:S(2)}) copy-start(bf16[1,512,2048]{2,1,0:T(8,128)(2,1)} %param.48) | copy-start | bytes 6291460
  7.2 5.8 %copy-start.4 = (bf16[2,2048]{1,0:T(2,128)(2,1)S(1)}, bf16[2,2048]{1,0:T(2,128)(2,1)}, u32[]{:S(2)}) copy-start(bf16[2,2048]{1,0:T(2,128)(2,1)} %param.26) | copy-start | bytes 24580
  7.2 5.8 %copy-start.5 = (f32[2048]{0:T(1024)S(1)}, f32[2048]{0:T(1024)}, u32[]{:S(2)}) copy-start(f32[2048]{0:T(1024)} %param.30) | copy-start | bytes 24580
  7.2 5.7 copy-start.14
  7.2 5.7 copy-start.13
  7.2 5.7 copy-start.20
  7.2 5.8 copy-start.19
  7.2 5.8 copy-start.21
  7.3 129.4 %all-gather.11.cloned.1.call-start = ((), (), s32[]{:S(2)}) async-start(), calls=%async_computation.5 | async-start | bytes 8454144 | tf_op jit(solution)/shard_map/all_gather | solution.py:21
  8.9 300.6 %all-gather.13.cloned.1.call-start = ((), (), s32[]{:S(2)}) async-start(), calls=%async_computation.6 | async-start | bytes 1179648 | tf_op jit(solution)/shard_map/all_gather | solution.py:28
  13.3 126.3 %copy-start.8 = (bf16[2,3,1024]{2,0,1:T(2,128)(2,1)S(1)}, bf16[2,3,1024]{2,0,1:T(2,128)(2,1)}, u32[]{:S(2)}) copy-start(bf16[2,3,1024]{2,0,1:T(2,128)(2,1)} %param.28) | copy-start | bytes 36868
  13.3 126.3 %copy-start.10 = (f32[4,1024]{1,0:T(4,128)S(1)}, f32[4,1024]{1,0:T(4,128)}, u32[]{:S(2)}) copy-start(f32[4,1024]{1,0:T(4,128)} %param.36) | copy-start | bytes 49156
  13.3 126.5 %copy-start.3 = (f32[2,16,64,128]{3,2,1,0:T(8,128)S(1)}, f32[2,16,64,128]{3,2,1,0:T(8,128)}, u32[]{:S(2)}) copy-start(f32[2,16,64,128]{3,2,1,0:T(8,128)} %param.27) | copy-start | bytes 3145732
  143.0 42.4 %copy-start.9 = (bf16[1024,16]{0,1:T(8,128)(2,1)S(1)}, bf16[1024,16]{0,1:T(8,128)(2,1)}, u32[]{:S(2)}) copy-start(bf16[1024,16]{0,1:T(8,128)(2,1)} %param.42) | copy-start | bytes 98308
  145.9 80.2 %copy-start.12 = (f32[2048]{0:T(1024)S(1)}, f32[2048]{0:T(1024)}, u32[]{:S(2)}) copy-start(f32[2048]{0:T(1024)} %param.43) | copy-start | bytes 24580
  145.9 99.7 %copy-start.7 = (bf16[16,2048]{1,0:T(8,128)(2,1)S(1)}, bf16[16,2048]{1,0:T(8,128)(2,1)}, u32[]{:S(2)}) copy-start(bf16[16,2048]{1,0:T(8,128)(2,1)} %param.50) | copy-start | bytes 196612
  146.0 109.3 %copy-start.18 = (bf16[2,4]{1,0:T(2,128)(2,1)S(1)}, bf16[2,4]{1,0:T(2,128)(2,1)}, u32[]{:S(2)}) copy-start(bf16[2,4]{1,0:T(2,128)(2,1)} %param.45) | copy-start | bytes 52
  146.0 115.1 %copy-start.16 = (s32[2,4]{1,0:T(2,128)S(1)}, s32[2,4]{1,0:T(2,128)}, u32[]{:S(2)}) copy-start(s32[2,4]{1,0:T(2,128)} %param.44) | copy-start | bytes 100
  246.3 89.4 %all-to-all-start.2 = ((bf16[16,2,1024]{2,0,1:T(8,128)(2,1)}), bf16[16,2,1024]{2,0,1:T(8,128)(2,1)S(1)}, u32[]{:S(2)}, u32[]{:S(2)}) async-start(bf16[16,2,1024]{2,0,1:T(8,128)(2,1)} %bitcast.94), calls=%async_computation.2 | async-start | bytes 131072 | tf_op jit(solution)/shard_map/all_to_all | solution.py:202
  255.2 85.6 %reduce-scatter.2.cloned.1.call-start = ((), (), s32[]{:S(2)}) async-start(), calls=%async_computation.7 | async-start | bytes 196608 | tf_op jit(solution)/shard_map/reduce_scatter | solution.py:207
  313.0 3.3 copy-start.1
  313.0 3.7 copy-start.11
  316.3 248.9 %all-reduce.3.cloned.1.call-start = ((), (), s32[]{:S(2)}) async-start(), calls=%async_computation.8 | async-start | bytes 2097152
  335.7 8.2 %copy-start.22 = (u32[256]{0:T(256)S(1)}, u32[256]{0:T(256)}, u32[]{:S(2)}) copy-start(u32[256]{0:T(256)} %constant.83) | copy-start | bytes 3076
  (4 other events, 10.8 us)
Sparse Core Ops, SparseCore 0:
  12.3 124.3 all-gather.10
  245.8 32.3 all-gather.12
  316.4 24.3 reduce-scatter.1
  346.0 219.1 all-reduce.2
where the time goes:
time: 583 us; the launch traced here: 582 us
  waiting for transfers between devices  348 us (60%)
  blocking collectives  178 us (31%)
  matrix products  21.9 us (4%)
  between operations  14.9 us (3%)
  starting transfers between devices  9.06 us (2%)
    unnamed x5, waiting for transfers between devices  219 us
    all_gather x1, waiting for transfers between devices, in_one_piece(): result = lax.all_gather(both, axis, axis=dim, tiled=True)  123 us
    all_gather x11, blocking collectives, gathered_by_axis(): nearer = lax.all_gather(shard, axes[-1], axis=dim, tiled=True)  111 us
    all_to_all x1, blocking collectives, sent_to_all(): return lax.all_to_all(copies, axis, split_axis=0, concat_axis=0, tiled=True)  20.4 us
    all_to_all x1, blocking collectives, local(): lax.all_to_all(column_block, EP, split_axis=0, concat_axis=1, tiled=True)  19.8 us
    all_gather x1, blocking collectives, local(): pair_inner = lax.all_gather(dense_inner, 'tp', axis=1, tiled=True)  17.9 us
  transfers between devices with their start and end apart: 5, of which 3 were waited for; matrix products, arithmetic and copies ran while one was open for 3% of the time, Pallas kernels for 0%

commit v1 on v0

v1 whole, which is shorter than its diff:
```python
import functools

import jax
import jax.numpy as jnp
from jax import lax
from jax.experimental import pallas as pl
from jax.experimental.pallas import tpu as pltpu
from jax.sharding import Mesh
from jax.sharding import PartitionSpec as P

EP = ("ep_0", "ep_1", "ep_2")
EP_TP = ("ep_0", "ep_1", "ep_2", "tp")
MESH = pl.DeviceIdType.MESH
F32 = jnp.float32
BF16 = jnp.bfloat16
norm_eps = 1e-05
clamp_limit = 7.0
glu_alpha = 1.702
highest = lax.Precision.HIGHEST
NZ, NY, NX = 8, 4, 4
NZY, NYX = NZ * NY, NY * NX


sigmoid = jax.nn.sigmoid
silu = jax.nn.silu


def softplus(v):
    return jnp.maximum(v, 0.0) + jnp.log1p(jnp.exp(-jnp.abs(v)))


def dot(a, b, ca=1, cb=0, precision=None):
    return lax.dot_general(
        a, b, (((ca,), (cb,)), ((), ())), precision=precision, preferred_element_type=F32
    )


def rms_scale(values, gain_vec):
    return values * lax.rsqrt(jnp.mean(values * values, axis=-1, keepdims=True) + norm_eps) * gain_vec


def layer_kernel(
    tokens, conv_state, conv_proj_state, first_gain, step_weight, conv_kernel, conv_proj_kernel,
    step_bias, log_rate, skip_gain, group_gain, out_weight, second_gain, routing, dense_up,
    dense_down, dense_gate,
    head_state, gate_weight, inner_weight, write_weight, read_weight, expert_gate, expert_up,
    expert_down,
    layer_out, inner_out, proj_out, state_out,
    hs, ww, rw, eg, eu, ed, wg, wi, nblk, tok, psend_i, psend_g, precv_i, precv_g, rts, wo, mx,
    osend, orecv, rows, ddp, dact, dactp, epart, epartp, tsum, prs, fsend, frecv,
    lsem, ssem, rsem, planesem,
):
    z, y, x, c = [lax.axis_index(n) for n in EP_TP]
    zy = z * NY + y
    yx = y * NX + x
    zc = z * 2 + c
    expert = zy * NX + x
    base = yx * NZ
    other = 1 - c
    partner = (z, y, x, other)

    def zy_dev(i):
        return (i // NY, i % NY, x, c)

    def yx_dev(i):
        return (z, i // NX, i % NX, c)

    def zc_dev(i):
        return (i // 2, y, x, i % 2)

    def send(src, dst, s, r, device):
        pltpu.make_async_remote_copy(
            src_ref=src, dst_ref=dst, send_sem=s, recv_sem=r, device_id=device, device_id_type=MESH
        ).start()

    def landed(ref, sem):
        pltpu.make_async_copy(ref, ref, sem).wait()

    def around(me, n, fn):
        def step(r, carry):
            fn((me + r) % n)
            return carry

        lax.fori_loop(1, n, step, 0)

    loads = [
        (write_weight, ww), (read_weight, rw), (head_state, hs), (expert_gate.at[0], eg),
        (expert_up.at[0], eu), (expert_down.at[0], ed), (gate_weight, wg.at[x]),
        (inner_weight, wi.at[x]),
    ]
    copies = [pltpu.make_async_copy(a, b, lsem.at[i]) for i, (a, b) in enumerate(loads)]
    for i in (7, 6, 0, 1, 2, 3, 4, 5):
        copies[i].start()

    barrier = pltpu.get_barrier_semaphore()

    def hello(device):
        pl.semaphore_signal(barrier, inc=1, device_id=device, device_id_type=MESH)

    around(zy, NZY, lambda i: hello(zy_dev(i)))
    around(yx, NYX, lambda i: hello(yx_dev(i)))
    around(z, NZ, lambda i: hello((i, y, x, other)))
    hello(partner)

    normed = rms_scale(tokens[...].astype(F32), first_gain[...]).astype(BF16)
    for b in range(16):
        nblk[b] = normed[:, b * 128 : (b + 1) * 128]
    tok[zy] = nblk[zy // 2]
    rts[base + z] = routing[...]
    wo[yx] = jnp.transpose(out_weight[...])

    pl.semaphore_wait(barrier, (NZY - 1) + (NYX - 1) + (NZ - 1) + 1)

    around(zy, NZY, lambda i: send(nblk.at[i // 2], tok.at[zy], ssem.at[0], rsem.at[0], zy_dev(i)))
    around(x, NX, lambda i: send(inner_weight, wi.at[x], ssem.at[1], rsem.at[1], (z, y, i, c)))
    around(x, NX, lambda i: send(gate_weight, wg.at[x], ssem.at[2], rsem.at[2], (z, y, i, c)))
    around(z, NZ, lambda i: send(rts.at[base + z], rts.at[base + z], ssem.at[3], rsem.at[3], (i, y, x, c)))

    copies[0].wait()
    copies[1].wait()
    write_proj = dot(normed, ww[...]).astype(BF16)
    read_proj = dot(normed, rw[...]).astype(BF16)
    step_raw = dot(normed, step_weight[...])
    proj_out[0] = write_proj
    proj_out[1] = read_proj

    copies[6].wait()
    copies[7].wait()
    landed(tok.at[pl.ds(0, NZY - 1)], rsem.at[0])
    landed(wi.at[pl.ds(0, NX - 1)], rsem.at[1])
    all_tok = tok.reshape(2 * NZY, 128)[...]
    low = (y % 2) == 0

    def padded(weight):
        zero = jnp.zeros_like(weight)
        return jnp.concatenate([jnp.where(low, weight, zero), jnp.where(low, zero, weight)], axis=0)

    psend_i.reshape(2 * NZY, 1024)[...] = dot(all_tok, padded(wi.reshape(64, 1024)[...])).astype(BF16)
    around(zy, NZY, lambda i: send(psend_i.at[i], precv_i.at[zy], ssem.at[4], rsem.at[4], zy_dev(i)))
    precv_i[zy] = psend_i[zy]
    landed(wg.at[pl.ds(0, NX - 1)], rsem.at[2])
    psend_g.reshape(2 * NZY, 1024)[...] = dot(all_tok, padded(wg.reshape(64, 1024)[...])).astype(BF16)
    around(zy, NZY, lambda i: send(psend_g.at[i], precv_g.at[zy], ssem.at[5], rsem.at[5], zy_dev(i)))
    precv_g[zy] = psend_g[zy]
    landed(rts.at[pl.ds(0, NZ - 1)], rsem.at[3])
    mine8 = pl.ds(base, NZ)
    around(yx, NYX, lambda i: send(rts.at[mine8], rts.at[mine8], ssem.at[6], rsem.at[6], yx_dev(i)))
    around(yx, NYX, lambda i: send(wo.at[yx], wo.at[yx], ssem.at[7], rsem.at[7], yx_dev(i)))
    send(dense_down.at[other], ddp, ssem.at[8], rsem.at[8], partner)

    cps = conv_proj_state[...].astype(F32)
    cpk = conv_proj_kernel[...]

    def conv_of(w, fresh):
        total = fresh.astype(F32) * cpk[3, w : w + 1]
        for i in range(3):
            total = total + cps[:, i, w, :] * cpk[i, w : w + 1]
        return silu(total)

    write_vec = conv_of(0, write_proj)
    read_vec = conv_of(1, read_proj)
    step_size = softplus(step_raw + step_bias[...])
    decay = jnp.exp(-jnp.exp(log_rate[...]) * step_size)
    head_of = lax.broadcasted_iota(jnp.int32, (16, 1024), 1) // 64
    spread = (head_of == lax.broadcasted_iota(jnp.int32, (16, 1024), 0)).astype(F32)
    step_wide = dot(step_size, spread, precision=highest)
    skip_wide = dot(skip_gain[...], spread, precision=highest)
    cs = conv_state[...].astype(F32)
    ck = conv_kernel[...]
    early = cs[:, 0, :] * ck[0:1] + cs[:, 1, :] * ck[1:2] + cs[:, 2, :] * ck[2:3]
    copies[2].wait()

    landed(precv_i.at[pl.ds(0, NZY - 1)], rsem.at[4])
    inner_proj = jnp.sum(precv_i[...].astype(F32), axis=0).astype(BF16)
    inner_out[...] = inner_proj
    conv_inner = silu(early + inner_proj.astype(F32) * ck[3:4])
    driven = step_wide * conv_inner
    first_row = lax.broadcasted_iota(jnp.int32, (8, 512), 0) == 0
    read_rows = []
    for s in range(2):
        for g in range(2):
            lhs = jnp.where(first_row, driven[s : s + 1, g * 512 : (g + 1) * 512], 0.0)
            rhs = jnp.broadcast_to(write_vec[s : s + 1, g * 128 : (g + 1) * 128], (8, 128))
            update = dot(lhs, rhs, 0, 0, highest).reshape(8, 64, 128)
            blocks = []
            for h in range(8):
                head = g * 8 + h
                rate = jnp.broadcast_to(decay[s : s + 1, head : head + 1], (64, 128))
                fresh = rate * hs[s, head] + update[h]
                hs[s, head] = fresh
                blocks.append(fresh)
            group = jnp.concatenate(blocks, axis=0)
            reader = jnp.broadcast_to(read_vec[s : s + 1, g * 128 : (g + 1) * 128], (8, 128))
            read_rows.append(dot(reader, group, 1, 1, highest)[0:1])
    state_copy = pltpu.make_async_copy(hs, state_out, lsem.at[2])
    state_copy.start()
    read_out = jnp.concatenate(
        [jnp.concatenate(read_rows[0:2], axis=1), jnp.concatenate(read_rows[2:4], axis=1)], axis=0
    ) + skip_wide * conv_inner

    landed(precv_g.at[pl.ds(0, NZY - 1)], rsem.at[5])
    gate_proj = jnp.sum(precv_g[...].astype(F32), axis=0).astype(BF16)
    gated = read_out * silu(gate_proj.astype(F32))
    parts = []
    for g in range(2):
        part = gated[:, g * 512 : (g + 1) * 512]
        parts.append(part * lax.rsqrt(jnp.mean(part * part, axis=-1, keepdims=True) + norm_eps))
    mx[z] = (jnp.concatenate(parts, axis=1) * group_gain[...]).astype(BF16)
    around(z, NZ, lambda i: send(mx.at[z], mx.at[z], ssem.at[9], rsem.at[9], (i, y, x, c)))

    landed(rts.at[pl.ds(0, 120)], rsem.at[6])
    table = rts.reshape(256, 256)[...].astype(F32)
    names, scores = table[:, 0:128], table[:, 128:256]
    lane = lax.broadcasted_iota(jnp.int32, (256, 128), 1)
    live = lane < 4
    hit = jnp.where(live & (names == expert.astype(F32)), 1.0, 0.0)
    shifted = jnp.where(live, scores, -3e38)
    grown = jnp.where(live, jnp.exp(shifted - jnp.max(shifted, axis=1, keepdims=True)), 0.0)
    row_weight = jnp.sum(hit * grown, axis=1, keepdims=True) / jnp.sum(grown, axis=1, keepdims=True)
    chosen = jnp.broadcast_to(jnp.sum(hit, axis=1, keepdims=True), (256, 128))
    rr = lax.broadcasted_iota(jnp.int32, (256, 256), 0)
    cc = lax.broadcasted_iota(jnp.int32, (256, 256), 1)
    chosen16 = chosen.astype(BF16)
    count_col = dot((cc <= rr).astype(BF16), chosen16)
    count_row = dot(chosen16, (rr <= cc).astype(BF16), 0, 0)[0:32]
    chosen_row = dot(chosen16, (rr == cc).astype(BF16), 0, 0)[0:32]
    slot = lax.broadcasted_iota(jnp.int32, (32, 256), 0).astype(F32)
    picks = jnp.where((count_row - 1.0 == slot) & (chosen_row > 0.5), 1.0, 0.0)
    picks_t = jnp.where((count_col - 1.0 == lane.astype(F32)) & (chosen > 0.5), 1.0, 0.0)
    slot_weight = dot(picks, jnp.broadcast_to(row_weight, (256, 128)), precision=highest)[:, 0:1]
    picks16 = picks.astype(BF16)

    landed(wo.at[pl.ds(0, NYX - 1)], rsem.at[7])
    landed(mx.at[pl.ds(0, NZ - 1)], rsem.at[9])
    osend.reshape(16, 256)[...] = dot(mx.reshape(16, 1024)[...], wo.reshape(256, 1024)[...], 1, 1)
    around(zc, 2 * NZ, lambda i: send(osend.at[i // 2], orecv.at[zc], ssem.at[10], rsem.at[10], zc_dev(i)))
    orecv[zc] = osend[z]
    landed(orecv.at[pl.ds(0, 15)], rsem.at[10])
    mixed = jnp.concatenate([orecv[2 * k] + orecv[2 * k + 1] for k in range(NZ)], axis=1)
    hidden = (tokens[...].astype(F32) + mixed).astype(BF16)
    normed_mid = rms_scale(hidden.astype(F32), second_gain[...]).astype(BF16)
    rows[c, base + z] = jnp.where(c == 0, normed_mid[:, 0:1024], normed_mid[:, 1024:2048])
    around(z, NZ, lambda i: send(rows.at[c, base + z], rows.at[c, base + z], ssem.at[11], rsem.at[11], (i, y, x, c)))
    landed(rows.at[c, pl.ds(0, NZ - 1)], rsem.at[11])
    around(yx, NYX, lambda i: send(rows.at[c, mine8], rows.at[c, mine8], ssem.at[12], planesem.at[yx], yx_dev(i)))
    send(rows.at[c, mine8], rows.at[c, mine8], ssem.at[13], rsem.at[13], partner)

    def forward(r, carry):
        i = (yx + NYX - r) % NYX
        block = rows.at[c, pl.ds(i * NZ, NZ)]
        landed(block, planesem.at[i])
        send(block, block, ssem.at[13], rsem.at[13], partner)
        return carry

    lax.fori_loop(1, NYX, forward, 0)
    copies[3].wait()
    copies[4].wait()
    copies[5].wait()
    landed(rows.at[other], rsem.at[13])

    halves = [rows[k].reshape(256, 1024) for k in range(2)]
    gate_line = dense_gate[...]
    g_hi = gate_line.astype(BF16)
    g_mid = (gate_line - g_hi.astype(F32)).astype(BF16)
    g_lo = (gate_line - g_hi.astype(F32) - g_mid.astype(F32)).astype(BF16)
    lines = jnp.concatenate([g_hi, g_mid, g_lo, jnp.zeros((5, 2048), BF16)], axis=0)
    picked = [dot(picks16, halves[k]).astype(BF16) for k in range(2)]
    gate_pre = dot(picked[0], eg[0:1024]) + dot(picked[1], eg[1024:2048])
    up_pre = dot(picked[0], eu[0:1024]) + dot(picked[1], eu[1024:2048])
    glu_part = jnp.minimum(gate_pre, clamp_limit)
    lin_part = jnp.clip(up_pre, -clamp_limit, clamp_limit)
    activated = (glu_part * sigmoid(glu_alpha * glu_part) * (lin_part + 1.0)).astype(BF16)
    part = dot(activated, ed[...]) * slot_weight
    epart[...] = jnp.where(c == 0, part[:, 1024:2048], part[:, 0:1024]).astype(BF16)
    send(epart, epartp, ssem.at[14], rsem.at[14], partner)
    own_part = jnp.where(c == 0, part[:, 0:1024], part[:, 1024:2048])
    up = dense_up[...]
    pre = dot(halves[0], up[0:1024]) + dot(halves[1], up[1024:2048])
    weigh = dot(halves[0], lines[:, 0:1024], 1, 1) + dot(halves[1], lines[:, 1024:2048], 1, 1)
    weight = sigmoid(jnp.sum(weigh, axis=1, keepdims=True))
    dense_act = silu(pre).astype(BF16).astype(F32) * weight
    dact[...] = dense_act.astype(BF16)
    send(dact, dactp, ssem.at[15], rsem.at[15], partner)
    landed(ddp, rsem.at[8])
    landed(epartp, rsem.at[14])
    both = (own_part + epartp[...].astype(F32)).astype(BF16)
    landed(dactp, rsem.at[15])
    left = jnp.concatenate([dact[...], dactp[...], picks_t[:, 0:32].astype(BF16)], axis=1)
    own_down = jnp.where(c == 0, dense_down[0], dense_down[1])
    right = jnp.concatenate([own_down, ddp[...], both], axis=0)
    tsum.reshape(256, 1024)[...] = dot(left, right).astype(BF16)

    around(yx, NYX, lambda i: send(tsum.at[pl.ds(i * NZ, NZ)], prs.at[yx], ssem.at[16], rsem.at[16], yx_dev(i)))
    prs[yx] = tsum[mine8]
    landed(prs.at[pl.ds(0, NYX - 1)], rsem.at[16])
    fsend[...] = jnp.sum(prs[...].astype(F32), axis=0).astype(BF16)
    around(zc, 2 * NZ, lambda i: send(fsend.at[i // 2], frecv.at[zc], ssem.at[17], rsem.at[17], zc_dev(i)))
    frecv[zc] = fsend[z]
    landed(frecv.at[pl.ds(0, 15)], rsem.at[17])
    final = []
    for k in range(2):
        total = frecv[k].astype(F32)
        for i in range(1, NZ):
            total = total + frecv[2 * i + k].astype(F32)
        final.append(total)
    result = hidden.astype(F32) + jnp.concatenate(final, axis=1)
    layer_out[...] = jnp.where(c == 0, result[0:1], result[1:2]).astype(BF16)

    state_copy.wait()
    for i, ref in enumerate((
        tok.at[pl.ds(0, NZY - 1)], wi.at[pl.ds(0, NX - 1)], wg.at[pl.ds(0, NX - 1)],
        rts.at[pl.ds(0, NZ - 1)], psend_i.at[pl.ds(0, NZY - 1)], psend_g.at[pl.ds(0, NZY - 1)],
        rts.at[pl.ds(0, 120)], wo.at[pl.ds(0, NYX - 1)], ddp, mx.at[pl.ds(0, NZ - 1)],
        orecv.at[pl.ds(0, 15)], mx.at[pl.ds(0, NZ - 1)], rows.at[0, pl.ds(0, 120)], rows.at[0],
        epart, dact, prs.at[pl.ds(0, NYX - 1)], frecv.at[pl.ds(0, 15)],
    )):
        landed(ref, ssem.at[i])


def local(
    tokens, head_state, conv_state, conv_proj_state, first_gain, gate_weight, inner_weight,
    write_weight, read_weight, step_weight, conv_kernel, conv_proj_kernel, step_bias, log_rate,
    skip_gain, group_gain, out_weight, second_gain, routes, route_logits, expert_gate, expert_up,
    expert_down, dense_up, dense_down, dense_gate,
):
    wide = ((0, 0), (0, 124))
    routing = jnp.concatenate(
        [jnp.pad(routes.astype(BF16), wide), jnp.pad(route_logits, wide)], axis=1
    )
    near = [
        tokens, conv_state, conv_proj_state, first_gain[None], step_weight, conv_kernel,
        conv_proj_kernel, step_bias[None], log_rate[None], skip_gain[None], group_gain[None],
        out_weight, second_gain[None], routing, dense_up,
        jnp.stack([dense_down[:, 0:1024], dense_down[:, 1024:2048]]), dense_gate[None],
    ]
    far = [
        head_state, gate_weight, inner_weight, write_weight, read_weight, expert_gate, expert_up,
        expert_down,
    ]
    vmem = pl.BlockSpec(memory_space=pltpu.VMEM)
    anywhere = pl.BlockSpec(memory_space=pl.ANY)
    V = pltpu.VMEM
    layer_out, inner_proj, proj, state_out = pl.pallas_call(
        layer_kernel,
        out_shape=(
            jax.ShapeDtypeStruct((1, 2048), BF16),
            jax.ShapeDtypeStruct((2, 1024), BF16),
            jax.ShapeDtypeStruct((2, 2, 256), BF16),
            jax.ShapeDtypeStruct((2, 16, 64, 128), F32),
        ),
        in_specs=[vmem] * len(near) + [anywhere] * len(far),
        out_specs=(vmem, vmem, vmem, anywhere),
        scratch_shapes=[
            V((2, 16, 64, 128), F32), V((2048, 256), BF16), V((2048, 256), BF16),
            V((2048, 512), BF16), V((2048, 512), BF16), V((512, 2048), BF16),
            V((NX, 16, 1024), BF16), V((NX, 16, 1024), BF16),
            V((16, 2, 128), BF16), V((NZY, 2, 128), BF16),
            V((NZY, 2, 1024), BF16), V((NZY, 2, 1024), BF16),
            V((NZY, 2, 1024), BF16), V((NZY, 2, 1024), BF16),
            V((128, 2, 256), BF16), V((NYX, 16, 1024), BF16), V((NZ, 2, 1024), BF16),
            V((NZ, 2, 256), F32), V((2 * NZ, 2, 256), F32),
            V((2, 128, 2, 1024), BF16), V((16, 1024), BF16), V((256, 16), BF16), V((256, 16), BF16),
            V((32, 1024), BF16), V((32, 1024), BF16),
            V((128, 2, 1024), BF16), V((NYX, NZ, 2, 1024), BF16), V((NZ, 2, 1024), BF16),
            V((2 * NZ, 2, 1024), BF16),
            pltpu.SemaphoreType.DMA((8,)), pltpu.SemaphoreType.DMA((18,)),
            pltpu.SemaphoreType.DMA((18,)), pltpu.SemaphoreType.DMA((NYX,)),
        ],
        compiler_params=pltpu.CompilerParams(
            collective_id=0, has_side_effects=True, vmem_limit_bytes=56 * 1024 * 1024
        ),
        cost_estimate=pl.CostEstimate(flops=2 * 10**9, bytes_accessed=16 * 2**20, transcendentals=10**5),
        name="layer",
    )(*near, *far)
    conv_out = jnp.concatenate([conv_state[:, 1:], inner_proj[:, None]], axis=1)
    conv_proj_out = jnp.concatenate(
        [conv_proj_state[:, 1:], jnp.stack([proj[0], proj[1]], axis=1)[:, None]], axis=1
    )
    return (layer_out, state_out, conv_out, conv_proj_out)


def solution(mesh):
    torus = Mesh(mesh.devices.reshape(NZ, NY, NX, mesh.shape["tp"]), EP_TP)
    return jax.shard_map(
        local,
        mesh=torus,
        in_specs=(
            P(EP, None), P(EP, "tp", None, None), P(EP, None, "tp"), P(EP, None, None, "tp"), P(),
            P(EP, "tp"), P(EP, "tp"), P(None, "tp"), P(None, "tp"), P(None, "tp"), P(None, "tp"),
            P(None, None, "tp"), P("tp"), P("tp"), P("tp"), P("tp"), P("tp", EP), P(), P(EP, None),
            P(EP, None), P(EP, None, "tp"), P(EP, None, "tp"), P(EP, "tp", None), P(None, EP_TP),
            P(EP_TP, None), P(),
        ),
        out_specs=(
            P(EP_TP, None), P(EP, "tp", None, None), P(EP, None, "tp"), P(EP, None, None, "tp"),
        ),
        check_vma=False,
    )
```

time: 583 us -> 92 us (0.16)
  waiting for transfers between devices: 348 us -> 0 us
  blocking collectives: 178 us -> 0 us
  Pallas kernels: 0 us -> 74.6 us
  matrix products: 21.9 us -> 0 us
  between operations: 14.9 us -> 0.66 us
  starting transfers between devices: 9.06 us -> 0 us
  local copies, waits for them, and re-layouts: 5.03 us -> 11.7 us
    unnamed x5 -> x0, waiting for transfers between devices: 219 us -> none
    all_gather x12 -> x0, blocking collectives: 129 us -> none  [the longest x11 111 us: gathered_by_axis(): nearer = lax.all_gather(shard, axes[-1], axis=dim, tiled=True)]
    all_gather x2 -> x0, waiting for transfers between devices: 123 us -> none  [the longest x1 123 us: in_one_piece(): result = lax.all_gather(both, axis, axis=dim, tiled=True)]
    pallas_call x0 -> x1, Pallas kernels: none -> 74.6 us  [local(): pl.pallas_call(layer_kernel, out_shape=(jax.ShapeDtypeStruct((1, 2048), B...]
    all_to_all x3 -> x0, blocking collectives: 48.8 us -> none  [the longest x1 20.4 us: sent_to_all(): return lax.all_to_all(copies, axis, split_axis=0, concat_axis=0, tiled=True)]
    dot_general x14 -> x0, matrix products: 21.9 us -> none  [the longest x1 3.23 us: local(): jnp.dot(activated, expert_down[0], preferred_element_type=jnp.float32)]
    all_to_all x1 -> x0, starting transfers between devices: 8.94 us -> none  [local(): lax.all_to_all(dense_down, 'tp', split_axis=1, concat_axis=0, tiled=True)]
    unnamed x56 -> x6, local copies, waits for them, and re-layouts: 2.15 us -> 10.2 us
  transfers between devices with their start and end apart: 5 -> 0, of which waited for: 3 -> 0; matrix products, arithmetic and copies ran while one was open for 3% -> 0% of each run, Pallas kernels for 0% -> 0%
where the time goes in v1:
time: 92 us; the launch traced here: 91.4 us
  Pallas kernels  74.6 us (81%)
  local copies, waits for them, and re-layouts  11.7 us (13%)
  other arithmetic  4.45 us (5%)
    pallas_call x1, Pallas kernels, local(): pl.pallas_call(layer_kernel, out_shape=(jax.ShapeDtypeStruct((1, 2048), B...  74.6 us
    unnamed x6, local copies, waits for them, and re-layouts  10.2 us

profile of v1, /device:TPU:1, one launch (start us, length us, event | category | flops | bytes accessed | tf_op | source)
XLA Modules:
  0.0 91.4 jit_solution(17509836092004111523)
XLA Ops:
  0.6 0.8 slice_bitcast_fusion.1
  1.4 0.6 pad_maximum_fusion.dense_down
  2.1 1.8 %copy.31.step_weight = bf16[2048,16]{1,0:T(8,128)(2,1)} copy(bf16[2048,16]{0,1:T(8,128)(2,1)} %param.35) | data formatting | bytes 131072 | tf_op args[9]
  3.9 1.8 %copy.33.dense_up = bf16[2048,16]{1,0:T(8,128)(2,1)} copy(bf16[2048,16]{0,1:T(8,128)(2,1)} %param.49) | data formatting | bytes 131072 | tf_op args[23]
  5.7 1.6 %copy.32.out_weight = bf16[1024,16]{1,0:T(8,128)(2,1)} copy(bf16[1024,16]{0,1:T(8,128)(2,1)} %param.42) | data formatting | bytes 65536 | tf_op args[16]
  7.3 1.3 %copy.30.conv_state = bf16[2,3,1024]{2,1,0:T(4,128)(2,1)} copy(bf16[2,3,1024]{2,0,1:T(2,128)(2,1)} %param.28) | data formatting | bytes 24576 | tf_op args[2]
  8.6 0.7 convert_element_type.6
  9.3 1.2 %fusion.routing = bf16[2,256]{1,0:T(2,128)(2,1)} fusion(bf16[2,4]{1,0:T(2,128)(2,1)} %param.45, bf16[2,4]{1,0:T(2,128)(2,1)S(1)} %convert_element_type.6), kind=kLoop, calls=%fused_computation.8 | loop fusion | flops 4096 | bytes 1056 | tf_op jit(solution)/shard_map/concatenate | solution.py:327
  10.5 0.0 slice-start.1
  10.5 0.0 slice-start
  10.5 74.6 %layer.1 = (bf16[1,2048]{1,0:T(2,128)(2,1)}, bf16[2,1024]{1,0:T(2,128)(2,1)}, bf16[2,2,256]{2,1,0:T(2,128)(2,1)}, f32[2,16,64,128]{3,2,1,0:T(8,128)}) custom-call(bf16[2,2048]{1,0:T(2,128)(2,1)} %tokens.1, bf16[2,3,1024]{2,1,0:T(4,128)(2,1)} %copy.30.conv_state, bf16[2,3,2,256]{3,2,1,0:T(2,128)(2,1)} %conv_proj_state.1, f32[1,2048]{1,0:T(1,128)} %bitcast.18, ...), custom_call_target="tpu_custom_call" | custom-call | flops 2000000000 | bytes 16777216 | tf_op jit(solution)/shard_map/layer/pallas_call | solution.py:343
  85.2 0.7 slice_bitcast_fusion.3
  85.9 0.0 slice-done.1
  85.9 0.6 pad_maximum_fusion.2
  86.5 0.0 slice-done
  86.5 1.3 %pad_maximum_fusion.1 = bf16[2,3,1024]{2,0,1:T(2,128)(2,1)} fusion(bf16[2,1,1024]{2,0,1:T(2,128)(2,1)} %bitcast.22, bf16[2,2,1024]{2,0,1:T(2,128)(2,1)S(1)} %slice-done), kind=kLoop, calls=%fused_computation.3 | loop fusion | flops 6144 | bytes 24576 | tf_op jit(solution)/shard_map/concatenate | solution.py:375
  87.8 1.3 %copy.37 = bf16[1,2048]{1,0:T(2,128)(2,1)} copy(bf16[1,2048]{1,0:T(2,128)(2,1)} %get-tuple-element.20) | data formatting | bytes 8192
  89.1 2.3 %copy.38 = f32[2,16,64,128]{3,2,1,0:T(8,128)} copy(f32[2,16,64,128]{3,2,1,0:T(8,128)} %get-tuple-element.21) | data formatting | bytes 2097152
  (2 shorter events, 0.0 us)
Async XLA Ops:
  10.5 75.4 %slice-start.1 = ((bf16[2,3,2,256]{3,2,1,0:T(2,128)(2,1)}), bf16[2,2,2,256]{3,2,1,0:T(2,128)(2,1)S(1)}, s32[]{:S(2)}) async-start(bf16[2,3,2,256]{3,2,1,0:T(2,128)(2,1)} %conv_proj_state.1), calls=%async_computation.1 | async-start | bytes 8192 | tf_op jit(solution)/shard_map/slice | solution.py:377
  10.5 76.0 %slice-start = ((bf16[2,3,1024]{2,0,1:T(2,128)(2,1)}), bf16[2,2,1024]{2,0,1:T(2,128)(2,1)S(1)}, s32[]{:S(2)}) async-start(bf16[2,3,1024]{2,0,1:T(2,128)(2,1)} %param.28), calls=%async_computation | async-start | bytes 16384 | tf_op jit(solution)/shard_map/slice | solution.py:375

commit v2 on v1

v2 whole, which is shorter than its diff:
```python
import functools

import jax
import jax.numpy as jnp
from jax import lax
from jax.experimental import pallas as pl
from jax.experimental.pallas import tpu as pltpu
from jax.sharding import Mesh
from jax.sharding import PartitionSpec as P

EP = ("ep_0", "ep_1", "ep_2")
EP_TP = ("ep_0", "ep_1", "ep_2", "tp")
MESH = pl.DeviceIdType.MESH
F32 = jnp.float32
BF16 = jnp.bfloat16
norm_eps = 1e-05
clamp_limit = 7.0
glu_alpha = 1.702
highest = lax.Precision.HIGHEST
NZ, NY, NX = 8, 4, 4
NZY, NYX = NZ * NY, NY * NX


sigmoid = jax.nn.sigmoid
silu = jax.nn.silu


def softplus(v):
    return jnp.maximum(v, 0.0) + jnp.log1p(jnp.exp(-jnp.abs(v)))


def dot(a, b, ca=1, cb=0, precision=None):
    return lax.dot_general(
        a, b, (((ca,), (cb,)), ((), ())), precision=precision, preferred_element_type=F32
    )


def rms_scale(values, gain_vec):
    return values * lax.rsqrt(jnp.mean(values * values, axis=-1, keepdims=True) + norm_eps) * gain_vec


NEAR = 17


def layer_kernel(*refs):
    near_hbm, refs = refs[:NEAR], refs[NEAR:]
    (
        out_weight, head_state, gate_weight, inner_weight, write_weight, read_weight, expert_gate,
        expert_up, expert_down, layer_out, conv_out, conv_proj_out, hs,
    ) = refs[:13]
    near, refs = refs[13 : 13 + NEAR], refs[13 + NEAR :]
    (
        tokens, first_gain, step_weight, conv_state, conv_proj_state, conv_kernel, conv_proj_kernel,
        step_bias, log_rate, skip_gain, group_gain, second_gain, routes, route_logits, dense_up,
        dense_down, dense_gate,
    ) = near
    (
        ww, rw, eg, eu, ed, wg, wi, nblk, tok, psend_i, psend_g, precv_i, precv_g, rts, wo, mx,
        osend, orecv, tkz, hid, rows, ddp, dact, dactp, epart, epartp, tsum, prs, fsend, frecv,
        nsem, lsem, ssem, rsem, planesem,
    ) = refs
    z, y, x, c = [lax.axis_index(n) for n in EP_TP]
    zy = z * NY + y
    yx = y * NX + x
    zc = z * 2 + c
    expert = zy * NX + x
    base = yx * NZ
    other = 1 - c
    partner = (z, y, x, other)

    def zy_dev(i):
        return (i // NY, i % NY, x, c)

    def yx_dev(i):
        return (z, i // NX, i % NX, c)

    def pair_dev(i):
        return (z, i // (2 * NX), (i // 2) % NX, i % 2)

    def zc_dev(i):
        return (i // 2, y, x, i % 2)

    def send(src, dst, s, r, device):
        pltpu.make_async_remote_copy(
            src_ref=src, dst_ref=dst, send_sem=s, recv_sem=r, device_id=device, device_id_type=MESH
        ).start()

    def landed(ref, sem, name="tail"):
        with jax.named_scope(name):
            pltpu.make_async_copy(ref, ref, sem).wait()

    def around(me, n, fn):
        def step(r, carry):
            fn((me + r) % n)
            return carry

        lax.fori_loop(1, n, step, 0)

    barrier = pltpu.get_barrier_semaphore()

    def hello(device):
        pl.semaphore_signal(barrier, inc=1, device_id=device, device_id_type=MESH)

    around(zy, NZY, lambda i: hello(zy_dev(i)))
    around(yx * 2 + c, 2 * NYX, lambda i: hello(pair_dev(i)))
    around(z, NZ, lambda i: hello((i, y, x, other)))

    small = [pltpu.make_async_copy(a, b, nsem.at[i]) for i, (a, b) in enumerate(zip(near_hbm, near))]
    loads = [
        (write_weight, ww), (read_weight, rw), (head_state, hs), (expert_gate.at[0], eg),
        (expert_up.at[0], eu), (expert_down.at[0], ed), (gate_weight, wg.at[x]),
        (inner_weight, wi.at[x]),
    ]
    copies = [pltpu.make_async_copy(a, b, lsem.at[i]) for i, (a, b) in enumerate(loads)]
    for copy in small:
        copy.start()
    for i in (7, 6, 0, 1, 2, 3, 4, 5):
        copies[i].start()
    small[0].wait()
    small[1].wait()

    normed = rms_scale(tokens[...].astype(F32), first_gain[...]).astype(BF16)
    for b in range(16):
        nblk[b] = normed[:, b * 128 : (b + 1) * 128]
    tok[zy] = nblk[zy // 2]
    tkz[z] = tokens[...]
    small[12].wait()
    small[13].wait()
    blank = jnp.zeros((2, 124), F32)
    rts[base + z] = jnp.concatenate(
        [routes[...].astype(F32), blank, route_logits[...].astype(F32), blank], axis=1
    ).astype(BF16)

    with jax.named_scope("barrier"):
        pl.semaphore_wait(barrier, (NZY - 1) + (2 * NYX - 1) + (NZ - 1))

    around(zy, NZY, lambda i: send(nblk.at[i // 2], tok.at[zy], ssem.at[0], rsem.at[0], zy_dev(i)))
    around(x, NX, lambda i: send(inner_weight, wi.at[x], ssem.at[1], rsem.at[1], (z, y, i, c)))
    around(x, NX, lambda i: send(gate_weight, wg.at[x], ssem.at[2], rsem.at[2], (z, y, i, c)))
    around(z, NZ, lambda i: send(rts.at[base + z], rts.at[base + z], ssem.at[3], rsem.at[3], (i, y, x, c)))
    around(z, NZ, lambda i: send(tkz.at[z], tkz.at[z], ssem.at[11], rsem.at[11], (i, y, x, c)))
    keeper = yx // 8
    place = wo.at[c, yx % 8]

    def columns(r, carry):
        i = (yx + r) % NYX
        send(out_weight, place, ssem.at[7], rsem.at[7], (z, i // NX, i % NX, keeper))
        return carry

    lax.fori_loop(1, NYX, columns, 0)

    @pl.when(keeper == c)
    def _():
        pltpu.make_async_copy(out_weight, place, rsem.at[7]).start()

    @pl.when(keeper != c)
    def _():
        send(out_weight, place, ssem.at[7], rsem.at[7], partner)

    for copy in small[2:12] + small[14:]:
        copy.wait()

    with jax.named_scope("ww"):
        copies[0].wait()
        copies[1].wait()
    write_proj = dot(normed, ww[...]).astype(BF16)
    read_proj = dot(normed, rw[...]).astype(BF16)
    step_raw = dot(normed, step_weight[...], 1, 1)

    copies[6].wait()
    copies[7].wait()
    landed(tok.at[pl.ds(0, NZY - 1)], rsem.at[0], "tok")
    landed(wi.at[pl.ds(0, NX - 1)], rsem.at[1], "wi")
    all_tok = tok.reshape(2 * NZY, 128)[...]
    low = (y % 2) == 0

    def padded(weight):
        zero = jnp.zeros_like(weight)
        return jnp.concatenate([jnp.where(low, weight, zero), jnp.where(low, zero, weight)], axis=0)

    psend_i.reshape(2 * NZY, 1024)[...] = dot(all_tok, padded(wi.reshape(64, 1024)[...])).astype(BF16)
    around(zy, NZY, lambda i: send(psend_i.at[i], precv_i.at[zy], ssem.at[4], rsem.at[4], zy_dev(i)))
    precv_i[zy] = psend_i[zy]
    landed(wg.at[pl.ds(0, NX - 1)], rsem.at[2], "wg")
    psend_g.reshape(2 * NZY, 1024)[...] = dot(all_tok, padded(wg.reshape(64, 1024)[...])).astype(BF16)
    around(zy, NZY, lambda i: send(psend_g.at[i], precv_g.at[zy], ssem.at[5], rsem.at[5], zy_dev(i)))
    precv_g[zy] = psend_g[zy]
    landed(rts.at[pl.ds(0, NZ - 1)], rsem.at[3], "rt_z")
    mine8 = pl.ds(base, NZ)
    around(yx, NYX, lambda i: send(rts.at[mine8], rts.at[mine8], ssem.at[6], rsem.at[6], yx_dev(i)))
    send(dense_down.at[:, pl.ds(pl.multiple_of(other * 1024, 1024), 1024)], ddp, ssem.at[8], rsem.at[8], partner)

    cps = conv_proj_state[...].astype(F32)
    cpk = conv_proj_kernel[...]

    def conv_of(w, fresh):
        total = fresh.astype(F32) * cpk[3, w : w + 1]
        for i in range(3):
            total = total + cps[:, i, w, :] * cpk[i, w : w + 1]
        return silu(total)

    write_vec = conv_of(0, write_proj)
    read_vec = conv_of(1, read_proj)
    step_size = softplus(step_raw + step_bias[...])
    decay = jnp.exp(-jnp.exp(log_rate[...]) * step_size)
    head_of = lax.broadcasted_iota(jnp.int32, (16, 1024), 1) // 64
    spread = (head_of == lax.broadcasted_iota(jnp.int32, (16, 1024), 0)).astype(F32)
    step_wide = dot(step_size, spread, precision=highest)
    skip_wide = dot(skip_gain[...], spread, precision=highest)
    decay_wide = dot(decay, spread, precision=highest)
    ck = conv_kernel[...]
    early = sum(conv_state[i].astype(F32) * ck[i : i + 1] for i in range(3))
    for i in range(2):
        conv_out[i] = conv_state[i + 1]
        conv_proj_out[:, i] = conv_proj_state[:, i + 1]
    for s in range(2):
        conv_proj_out[s, 2] = jnp.concatenate([write_proj[s : s + 1], read_proj[s : s + 1]], axis=0)
    copies[2].wait()
    held, met = [], []
    for s in range(2):
        for g in range(2):
            span = slice(g * 128, (g + 1) * 128)
            reader = read_vec[s : s + 1, span]
            group = hs[s, g * 8 : (g + 1) * 8].reshape(512, 128)
            held.append(dot(jnp.broadcast_to(reader, (8, 128)), group, 1, 1, highest)[0:1])
            product = jnp.sum(write_vec[s : s + 1, span] * reader, axis=1, keepdims=True)
            met.append(jnp.broadcast_to(product, (1, 512)))

    def by_sequence(four):
        return jnp.concatenate(
            [jnp.concatenate(four[0:2], axis=1), jnp.concatenate(four[2:4], axis=1)], axis=0
        )

    kept = decay_wide * by_sequence(held)
    direct = step_wide * by_sequence(met) + skip_wide

    landed(precv_i.at[pl.ds(0, NZY - 1)], rsem.at[4], "p_inner")
    inner_proj = jnp.sum(precv_i[...].astype(F32), axis=0).astype(BF16)
    conv_out[2] = inner_proj
    conv_inner = silu(early + inner_proj.astype(F32) * ck[3:4])
    read_out = kept + direct * conv_inner

    landed(precv_g.at[pl.ds(0, NZY - 1)], rsem.at[5], "p_gate")
    gate_proj = jnp.sum(precv_g[...].astype(F32), axis=0).astype(BF16)
    gated = read_out * silu(gate_proj.astype(F32))
    parts = []
    for g in range(2):
        part = gated[:, g * 512 : (g + 1) * 512]
        parts.append(part * lax.rsqrt(jnp.mean(part * part, axis=-1, keepdims=True) + norm_eps))
    mx[c, z] = (jnp.concatenate(parts, axis=1) * group_gain[...]).astype(BF16)
    around(zc, 2 * NZ, lambda i: send(mx.at[c, z], mx.at[c, z], ssem.at[9], rsem.at[9], zc_dev(i)))

    landed(rts.at[pl.ds(0, 120)], rsem.at[6], "rt_yx")
    table = rts.reshape(256, 256)[...].astype(F32)
    names, scores = table[:, 0:128], table[:, 128:256]
    lane = lax.broadcasted_iota(jnp.int32, (256, 128), 1)
    live = lane < 4
    hit = jnp.where(live & (names == expert.astype(F32)), 1.0, 0.0)
    shifted = jnp.where(live, scores, -3e38)
    grown = jnp.where(live, jnp.exp(shifted - jnp.max(shifted, axis=1, keepdims=True)), 0.0)
    row_weight = jnp.sum(hit * grown, axis=1, keepdims=True) / jnp.sum(grown, axis=1, keepdims=True)
    chosen = jnp.broadcast_to(jnp.sum(hit, axis=1, keepdims=True), (256, 128))
    rr = lax.broadcasted_iota(jnp.int32, (256, 256), 0)
    cc = lax.broadcasted_iota(jnp.int32, (256, 256), 1)
    chosen16 = chosen.astype(BF16)
    count_col = dot((cc <= rr).astype(BF16), chosen16)
    count_row = dot(chosen16, (rr <= cc).astype(BF16), 0, 0)[0:32]
    chosen_row = dot(chosen16, (rr == cc).astype(BF16), 0, 0)[0:32]
    slot = lax.broadcasted_iota(jnp.int32, (32, 256), 0).astype(F32)
    picks = jnp.where((count_row - 1.0 == slot) & (chosen_row > 0.5), 1.0, 0.0)
    picks_t = jnp.where((count_col - 1.0 == lane.astype(F32)) & (chosen > 0.5), 1.0, 0.0)
    slot_weight = dot(picks, jnp.broadcast_to(row_weight, (256, 128)), precision=highest)[:, 0:1]
    picks16 = picks.astype(BF16)

    landed(wo, rsem.at[7], "wo")
    landed(frecv.at[pl.ds(0, 15)], rsem.at[9], "mixer")
    columns_out = [dot(mx[k].reshape(16, 1024), wo[k].reshape(128, 1024), 1, 1) for k in range(2)]
    osend[...] = (columns_out[0] + columns_out[1]).astype(BF16)
    around(zc, 2 * NZ, lambda i: send(osend, orecv.at[zc], ssem.at[10], rsem.at[10], zc_dev(i)))
    orecv[zc] = osend[...]
    landed(tkz.at[pl.ds(0, NZ - 1)], rsem.at[11], "tkz")
    landed(orecv.at[pl.ds(0, 15)], rsem.at[10], "out")
    mixed = jnp.concatenate([orecv[k].astype(F32) for k in range(2 * NZ)], axis=1)
    hidden = (tkz[...].reshape(16, 2048).astype(F32) + mixed).astype(BF16)
    hid[...] = hidden.reshape(NZ, 2, 2048)
    normed_mid = rms_scale(hidden.astype(F32), second_gain[...]).astype(BF16)
    for k in range(2):
        rows[k, mine8] = normed_mid[:, k * 1024 : (k + 1) * 1024].reshape(NZ, 2, 1024)
    around(yx, NYX, lambda i: send(rows.at[c, mine8], rows.at[c, mine8], ssem.at[12], planesem.at[yx], yx_dev(i)))

    driven = step_wide * conv_inner
    first_row = lax.broadcasted_iota(jnp.int32, (8, 512), 0) == 0
    for s in range(2):
        for g in range(2):
            lhs = jnp.where(first_row, driven[s : s + 1, g * 512 : (g + 1) * 512], 0.0)
            rhs = jnp.broadcast_to(write_vec[s : s + 1, g * 128 : (g + 1) * 128], (8, 128))
            update = dot(lhs, rhs, 0, 0, highest).reshape(8, 64, 128)
            for h in range(8):
                head = g * 8 + h
                rate = jnp.broadcast_to(decay[s : s + 1, head : head + 1], (64, 128))
                hs[s, head] = rate * hs[s, head] + update[h]

    def forward(r, carry):
        i = (yx + NYX - r) % NYX
        block = rows.at[c, pl.ds(i * NZ, NZ)]
        landed(block, planesem.at[i], "rows_yx")
        send(block, block, ssem.at[13], rsem.at[13], partner)
        return carry

    lax.fori_loop(1, NYX, forward, 0)
    copies[3].wait()
    copies[4].wait()
    copies[5].wait()

    gate_line = dense_gate[...]
    g_hi = gate_line.astype(BF16)
    g_mid = (gate_line - g_hi.astype(F32)).astype(BF16)
    g_lo = (gate_line - g_hi.astype(F32) - g_mid.astype(F32)).astype(BF16)
    lines = jnp.concatenate([g_hi, g_mid, g_lo, jnp.zeros((5, 2048), BF16)], axis=0)
    lines = jnp.stack([lines[:, 0:1024], lines[:, 1024:2048]])

    def half_terms(k):
        half = rows[k].reshape(256, 1024)
        span = pl.ds(pl.multiple_of(k * 1024, 1024), 1024)
        picked = dot(picks16, half).astype(BF16)
        line = jnp.where(k == 0, lines[0], lines[1])
        return (
            dot(picked, eg[span]), dot(picked, eu[span]), dot(half, dense_up[:, span], 1, 1),
            dot(half, line, 1, 1),
        )

    own_terms = half_terms(c)
    landed(rows.at[other, pl.ds(0, 120)], rsem.at[13], "rows_d2d")
    gate_pre, up_pre, pre, weigh = [a + b for a, b in zip(own_terms, half_terms(other))]
    glu_part = jnp.minimum(gate_pre, clamp_limit)
    lin_part = jnp.clip(up_pre, -clamp_limit, clamp_limit)
    activated = (glu_part * sigmoid(glu_alpha * glu_part) * (lin_part + 1.0)).astype(BF16)
    part = dot(activated, ed[...]) * slot_weight
    epart[...] = jnp.where(c == 0, part[:, 1024:2048], part[:, 0:1024]).astype(BF16)
    send(epart, epartp, ssem.at[14], rsem.at[14], partner)
    own_part = jnp.where(c == 0, part[:, 0:1024], part[:, 1024:2048])
    weight = sigmoid(jnp.sum(weigh, axis=1, keepdims=True))
    dense_act = silu(pre).astype(BF16).astype(F32) * weight
    dact[...] = dense_act.astype(BF16)
    send(dact, dactp, ssem.at[15], rsem.at[15], partner)
    landed(ddp, rsem.at[8], "ddp")
    landed(epartp, rsem.at[14], "epart")
    both = (own_part + epartp[...].astype(F32)).astype(BF16)
    landed(dactp, rsem.at[15], "dact")
    left = jnp.concatenate([dact[...], dactp[...], picks_t[:, 0:32].astype(BF16)], axis=1)
    own_down = jnp.where(c == 0, dense_down[:, 0:1024], dense_down[:, 1024:2048])
    right = jnp.concatenate([own_down, ddp[...], both], axis=0)
    tsum.reshape(256, 1024)[...] = dot(left, right).astype(BF16)

    around(yx, NYX, lambda i: send(tsum.at[pl.ds(i * NZ, NZ)], prs.at[yx], ssem.at[16], rsem.at[16], yx_dev(i)))
    prs[yx] = tsum[mine8]
    landed(prs.at[pl.ds(0, NYX - 1)], rsem.at[16], "sum_yx")
    fsend[...] = jnp.sum(prs[...].astype(F32), axis=0).astype(BF16)
    around(zc, 2 * NZ, lambda i: send(fsend.at[i // 2], frecv.at[zc], ssem.at[17], rsem.at[17], zc_dev(i)))
    frecv[zc] = fsend[z]
    landed(frecv.at[pl.ds(0, 15)], rsem.at[17], "sum_z")
    final = []
    for k in range(2):
        total = frecv[k].astype(F32)
        for i in range(1, NZ):
            total = total + frecv[2 * i + k].astype(F32)
        final.append(total)
    result = hid[z].astype(F32) + jnp.concatenate(final, axis=1)
    layer_out[...] = jnp.where(c == 0, result[0:1], result[1:2]).astype(BF16)

    for i, ref in enumerate((
        tok.at[pl.ds(0, NZY - 1)], wi.at[pl.ds(0, NX - 1)], wg.at[pl.ds(0, NX - 1)],
        rts.at[pl.ds(0, NZ - 1)], psend_i.at[pl.ds(0, NZY - 1)], psend_g.at[pl.ds(0, NZY - 1)],
        rts.at[pl.ds(0, 120)], None, ddp, frecv.at[pl.ds(0, 15)],
        orecv.at[pl.ds(0, 15)], tkz.at[pl.ds(0, NZ - 1)], rows.at[0, pl.ds(0, 120)],
        rows.at[0, pl.ds(0, 120)],
        epart, dact, prs.at[pl.ds(0, NYX - 1)], frecv.at[pl.ds(0, 15)],
    )):
        if ref is not None:
            landed(ref, ssem.at[i])

    @pl.when(keeper == c)
    def _():
        landed(prs.at[pl.ds(0, NYX - 1)], ssem.at[7])

    @pl.when(keeper != c)
    def _():
        landed(wo, ssem.at[7])


def local(
    tokens, head_state, conv_state, conv_proj_state, first_gain, gate_weight, inner_weight,
    write_weight, read_weight, step_weight, conv_kernel, conv_proj_kernel, step_bias, log_rate,
    skip_gain, group_gain, out_weight, second_gain, routes, route_logits, expert_gate, expert_up,
    expert_down, dense_up, dense_down, dense_gate,
):
    near = [
        tokens, first_gain[None], step_weight.T, conv_state.transpose(1, 0, 2), conv_proj_state,
        conv_kernel, conv_proj_kernel, step_bias[None], log_rate[None], skip_gain[None],
        group_gain[None], second_gain[None], routes, route_logits, dense_up.T, dense_down,
        dense_gate[None],
    ]
    far = [
        out_weight.T, head_state, gate_weight, inner_weight, write_weight, read_weight, expert_gate,
        expert_up, expert_down,
    ]
    vmem = pl.BlockSpec(memory_space=pltpu.VMEM)
    anywhere = pl.BlockSpec(memory_space=pltpu.HBM)
    V = pltpu.VMEM
    outs = (
        jax.ShapeDtypeStruct((1, 2048), BF16),
        jax.ShapeDtypeStruct((3, 2, 1024), BF16),
        jax.ShapeDtypeStruct((2, 3, 2, 256), BF16),
        jax.ShapeDtypeStruct((2, 16, 64, 128), F32),
    )
    layer_out, conv_out, conv_proj_out, state_out = pl.pallas_call(
        layer_kernel,
        out_shape=tuple(V(o.shape, o.dtype) for o in outs),
        in_specs=[anywhere] * (len(near) + len(far)),
        out_specs=(vmem, vmem, vmem, vmem),
        scratch_shapes=[
            *[V(a.shape, a.dtype) for a in near],
            V((2048, 256), BF16), V((2048, 256), BF16),
            V((2048, 512), BF16), V((2048, 512), BF16), V((512, 2048), BF16),
            V((NX, 16, 1024), BF16), V((NX, 16, 1024), BF16),
            V((16, 2, 128), BF16), V((NZY, 2, 128), BF16),
            V((NZY, 2, 1024), BF16), V((NZY, 2, 1024), BF16),
            V((NZY, 2, 1024), BF16), V((NZY, 2, 1024), BF16),
            V((128, 2, 256), BF16), V((2, 8, 16, 1024), BF16), V((2, NZ, 2, 1024), BF16),
            V((16, 128), BF16), V((2 * NZ, 16, 128), BF16), V((NZ, 2, 2048), BF16), V((NZ, 2, 2048), BF16),
            V((2, 128, 2, 1024), BF16), V((16, 1024), BF16), V((256, 16), BF16), V((256, 16), BF16),
            V((32, 1024), BF16), V((32, 1024), BF16),
            V((128, 2, 1024), BF16), V((NYX, NZ, 2, 1024), BF16), V((NZ, 2, 1024), BF16),
            V((2 * NZ, 2, 1024), BF16),
            pltpu.SemaphoreType.DMA((NEAR,)), pltpu.SemaphoreType.DMA((8,)), pltpu.SemaphoreType.DMA((18,)),
            pltpu.SemaphoreType.DMA((18,)), pltpu.SemaphoreType.DMA((NYX,)),
        ],
        compiler_params=pltpu.CompilerParams(
            collective_id=0, has_side_effects=True, vmem_limit_bytes=56 * 1024 * 1024
        ),
        cost_estimate=pl.CostEstimate(flops=2 * 10**9, bytes_accessed=16 * 2**20, transcendentals=10**5),
        name="layer",
    )(*near, *far)
    return (layer_out, state_out, conv_out.transpose(1, 0, 2), conv_proj_out)


def solution(mesh):
    torus = Mesh(mesh.devices.reshape(NZ, NY, NX, mesh.shape["tp"]), EP_TP)
    return jax.shard_map(
        local,
        mesh=torus,
        in_specs=(
            P(EP, None), P(EP, "tp", None, None), P(EP, None, "tp"), P(EP, None, None, "tp"), P(),
            P(EP, "tp"), P(EP, "tp"), P(None, "tp"), P(None, "tp"), P(None, "tp"), P(None, "tp"),
            P(None, None, "tp"), P("tp"), P("tp"), P("tp"), P("tp"), P("tp", EP), P(), P(EP, None),
            P(EP, None), P(EP, None, "tp"), P(EP, None, "tp"), P(EP, "tp", None), P(None, EP_TP),
            P(EP_TP, None), P(),
        ),
        out_specs=(
            P(EP_TP, None), P(EP, "tp", None, None), P(EP, None, "tp"), P(EP, None, None, "tp"),
        ),
        check_vma=False,
    )
```

time: 92 us -> 69.9 us (0.76)
  local copies, waits for them, and re-layouts: 11.7 us -> 2.76 us
  Pallas kernels: 74.6 us -> 66.4 us
  other arithmetic: 4.45 us -> 0 us
    pallas_call x1, Pallas kernels: 74.6 us -> 66.4 us  [local(): pl.pallas_call(layer_kernel, out_shape=tuple((V(o.shape, o.dtype) for o i...]
    unnamed x6 -> x4, local copies, waits for them, and re-layouts: 10.2 us -> 2.76 us
    concatenate x3 -> x0, other arithmetic: 3.12 us -> none  [the longest x1 1.29 us: local(): conv_out = jnp.concatenate([conv_state[:, 1:], inner_proj[:, None]], axis=1)]
    another operation x2 -> x0, local copies, waits for them, and re-layouts: 1.47 us -> none  [the longest x1 0.78 us: local(): jnp.stack([dense_down[:, 0:1024], dense_down[:, 1024:2048]])]
where the time goes in v2:
time: 69.9 us; the launch traced here: 69.8 us
  Pallas kernels  66.4 us (95%)
  local copies, waits for them, and re-layouts  2.76 us (4%)
    pallas_call x1, Pallas kernels, local(): pl.pallas_call(layer_kernel, out_shape=tuple((V(o.shape, o.dtype) for o i...  66.4 us
    unnamed x4, local copies, waits for them, and re-layouts  2.76 us

profile of v2, /device:TPU:1, one launch (start us, length us, event | category | flops | bytes accessed | tf_op | source)
XLA Modules:
  0.0 69.8 jit_solution(13747517267166583417)
XLA Ops:
  0.6 66.4 %layer.1 = (bf16[1,2048]{1,0:T(2,128)(2,1)S(1)}, bf16[3,2,1024]{2,1,0:T(2,128)(2,1)S(1)}, bf16[2,3,2,256]{3,2,1,0:T(2,128)(2,1)S(1)}, f32[2,16,64,128]{3,2,1,0:T(8,128)S(1)}) custom-call(bf16[2,2048]{1,0:T(2,128)(2,1)} %refs_0_.1, f32[1,2048]{1,0:T(1,128)} %bitcast.17, bf16[16,2048]{1,0:T(8,128)(2,1)} %bitcast.13, bf16[3,2,1024]{2,1,0:T(2,128)(2,1)} %bitcast.16, ...), custom_call_target="tpu_custom_call" | custom-call | flops 2000000000 | bytes 16777216 | tf_op jit(solution)/shard_map/layer/pallas_call | solution.py:416
  67.0 0.6 copy.34
  67.6 0.6 copy.37
  68.2 0.6 copy.36
  68.8 1.0 %copy.35 = f32[2,16,64,128]{3,2,1,0:T(8,128)} copy(f32[2,16,64,128]{3,2,1,0:T(8,128)S(1)} %get-tuple-element.13) | data formatting | bytes 2097152

commit v3 on v2

--- a/solution.py
+++ b/solution.py
@@ -57,7 +57,7 @@
     (
         ww, rw, eg, eu, ed, wg, wi, nblk, tok, psend_i, psend_g, precv_i, precv_g, rts, wo, mx,
         osend, orecv, tkz, hid, rows, ddp, dact, dactp, epart, epartp, tsum, prs, fsend, frecv,
-        nsem, lsem, ssem, rsem, planesem,
+        pt, upl, pbuf, dterm, nsem, lsem, ssem, rsem, planesem, fsem,
     ) = refs
     z, y, x, c = [lax.axis_index(n) for n in EP_TP]
     zy = z * NY + y
@@ -68,17 +68,14 @@
     other = 1 - c
     partner = (z, y, x, other)
 
-    def zy_dev(i):
-        return (i // NY, i % NY, x, c)
-
-    def yx_dev(i):
-        return (z, i // NX, i % NX, c)
-
-    def pair_dev(i):
-        return (z, i // (2 * NX), (i // 2) % NX, i % 2)
-
-    def zc_dev(i):
-        return (i // 2, y, x, i % 2)
+    z_at = [lax.rem(z + d, NZ) for d in range(NZ)]
+    y_at = [lax.rem(y + d, NY) for d in range(NY)]
+    x_at = [lax.rem(x + d, NX) for d in range(NX)]
+    c_at = [c, other]
+    zy_peers = [(z_at[d], y_at[e]) for d in (4, 3, 5, 2, 6, 1, 7, 0) for e in (2, 1, 3, 0)][:-1]
+    yx_peers = [(y_at[d], x_at[e]) for d in (2, 1, 3, 0) for e in (2, 1, 3, 0)][:-1]
+    zc_peers = [(z_at[d], c_at[e]) for d in (4, 3, 5, 2, 6, 1, 7, 0) for e in (1, 0)][:-1]
+    z_peers = [z_at[d] for d in (4, 3, 5, 2, 6, 1, 7)]
 
     def send(src, dst, s, r, device):
         pltpu.make_async_remote_copy(
@@ -89,21 +86,19 @@
         with jax.named_scope(name):
             pltpu.make_async_copy(ref, ref, sem).wait()
 
-    def around(me, n, fn):
-        def step(r, carry):
-            fn((me + r) % n)
-            return carry
-
-        lax.fori_loop(1, n, step, 0)
-
     barrier = pltpu.get_barrier_semaphore()
 
     def hello(device):
         pl.semaphore_signal(barrier, inc=1, device_id=device, device_id_type=MESH)
 
-    around(zy, NZY, lambda i: hello(zy_dev(i)))
-    around(yx * 2 + c, 2 * NYX, lambda i: hello(pair_dev(i)))
-    around(z, NZ, lambda i: hello((i, y, x, other)))
+    for k, j in zy_peers:
+        hello((k, j, x, c))
+    for j, i in yx_peers:
+        hello((z, j, i, c))
+        hello((z, j, i, other))
+    hello(partner)
+    for k in z_peers:
+        hello((k, y, x, other))
 
     small = [pltpu.make_async_copy(a, b, nsem.at[i]) for i, (a, b) in enumerate(zip(near_hbm, near))]
     loads = [
@@ -134,20 +129,21 @@
     with jax.named_scope("barrier"):
         pl.semaphore_wait(barrier, (NZY - 1) + (2 * NYX - 1) + (NZ - 1))
 
-    around(zy, NZY, lambda i: send(nblk.at[i // 2], tok.at[zy], ssem.at[0], rsem.at[0], zy_dev(i)))
-    around(x, NX, lambda i: send(inner_weight, wi.at[x], ssem.at[1], rsem.at[1], (z, y, i, c)))
-    around(x, NX, lambda i: send(gate_weight, wg.at[x], ssem.at[2], rsem.at[2], (z, y, i, c)))
-    around(z, NZ, lambda i: send(rts.at[base + z], rts.at[base + z], ssem.at[3], rsem.at[3], (i, y, x, c)))
-    around(z, NZ, lambda i: send(tkz.at[z], tkz.at[z], ssem.at[11], rsem.at[11], (i, y, x, c)))
+    for k, j in zy_peers:
+        send(nblk.at[k * 2 + j // 2], tok.at[zy], ssem.at[0], rsem.at[0], (k, j, x, c))
+    for k in z_peers:
+        send(rts.at[base + z], rts.at[base + z], ssem.at[3], rsem.at[3], (k, y, x, c))
+    for i in (x_at[2], x_at[1], x_at[3]):
+        send(inner_weight, wi.at[x], ssem.at[1], rsem.at[1], (z, y, i, c))
+    for i in (x_at[2], x_at[1], x_at[3]):
+        send(gate_weight, wg.at[x], ssem.at[2], rsem.at[2], (z, y, i, c))
+    for k in z_peers:
+        send(tkz.at[z], tkz.at[z], ssem.at[11], rsem.at[11], (k, y, x, c))
     keeper = yx // 8
     place = wo.at[c, yx % 8]
 
-    def columns(r, carry):
-        i = (yx + r) % NYX
-        send(out_weight, place, ssem.at[7], rsem.at[7], (z, i // NX, i % NX, keeper))
-        return carry
-
-    lax.fori_loop(1, NYX, columns, 0)
+    for j, i in yx_peers:
+        send(out_weight, place, ssem.at[7], rsem.at[7], (z, j, i, keeper))
 
     @pl.when(keeper == c)
     def _():
@@ -170,6 +166,10 @@
     copies[6].wait()
     copies[7].wait()
     landed(tok.at[pl.ds(0, NZY - 1)], rsem.at[0], "tok")
+    landed(rts.at[pl.ds(0, NZ - 1)], rsem.at[3], "rt_z")
+    mine8 = pl.ds(base, NZ)
+    for j, i in yx_peers:
+        send(rts.at[mine8], rts.at[mine8], ssem.at[6], rsem.at[6], (z, j, i, c))
     landed(wi.at[pl.ds(0, NX - 1)], rsem.at[1], "wi")
     all_tok = tok.reshape(2 * NZY, 128)[...]
     low = (y % 2) == 0
@@ -179,15 +179,14 @@
         return jnp.concatenate([jnp.where(low, weight, zero), jnp.where(low, zero, weight)], axis=0)
 
     psend_i.reshape(2 * NZY, 1024)[...] = dot(all_tok, padded(wi.reshape(64, 1024)[...])).astype(BF16)
-    around(zy, NZY, lambda i: send(psend_i.at[i], precv_i.at[zy], ssem.at[4], rsem.at[4], zy_dev(i)))
+    for k, j in zy_peers:
+        send(psend_i.at[k * NY + j], precv_i.at[zy], ssem.at[4], rsem.at[4], (k, j, x, c))
     precv_i[zy] = psend_i[zy]
     landed(wg.at[pl.ds(0, NX - 1)], rsem.at[2], "wg")
     psend_g.reshape(2 * NZY, 1024)[...] = dot(all_tok, padded(wg.reshape(64, 1024)[...])).astype(BF16)
-    around(zy, NZY, lambda i: send(psend_g.at[i], precv_g.at[zy], ssem.at[5], rsem.at[5], zy_dev(i)))
+    for k, j in zy_peers:
+        send(psend_g.at[k * NY + j], precv_g.at[zy], ssem.at[5], rsem.at[5], (k, j, x, c))
     precv_g[zy] = psend_g[zy]
-    landed(rts.at[pl.ds(0, NZ - 1)], rsem.at[3], "rt_z")
-    mine8 = pl.ds(base, NZ)
-    around(yx, NYX, lambda i: send(rts.at[mine8], rts.at[mine8], ssem.at[6], rsem.at[6], yx_dev(i)))
     send(dense_down.at[:, pl.ds(pl.multiple_of(other * 1024, 1024), 1024)], ddp, ssem.at[8], rsem.at[8], partner)
 
     cps = conv_proj_state[...].astype(F32)
@@ -248,7 +247,8 @@
         part = gated[:, g * 512 : (g + 1) * 512]
         parts.append(part * lax.rsqrt(jnp.mean(part * part, axis=-1, keepdims=True) + norm_eps))
     mx[c, z] = (jnp.concatenate(parts, axis=1) * group_gain[...]).astype(BF16)
-    around(zc, 2 * NZ, lambda i: send(mx.at[c, z], mx.at[c, z], ssem.at[9], rsem.at[9], zc_dev(i)))
+    for k, e in zc_peers:
+        send(mx.at[c, z], mx.at[c, z], ssem.at[9], rsem.at[9], (k, y, x, e))
 
     landed(rts.at[pl.ds(0, 120)], rsem.at[6], "rt_yx")
     table = rts.reshape(256, 256)[...].astype(F32)
@@ -270,13 +270,21 @@
     picks = jnp.where((count_row - 1.0 == slot) & (chosen_row > 0.5), 1.0, 0.0)
     picks_t = jnp.where((count_col - 1.0 == lane.astype(F32)) & (chosen > 0.5), 1.0, 0.0)
     slot_weight = dot(picks, jnp.broadcast_to(row_weight, (256, 128)), precision=highest)[:, 0:1]
-    picks16 = picks.astype(BF16)
+    pt[...] = picks_t.astype(BF16)
+    gate_line = dense_gate[...]
+    g_hi = gate_line.astype(BF16)
+    g_mid = (gate_line - g_hi.astype(F32)).astype(BF16)
+    g_lo = (gate_line - g_hi.astype(F32) - g_mid.astype(F32)).astype(BF16)
+    lines = jnp.concatenate([dense_up[...], g_hi, g_mid, g_lo, jnp.zeros((13, 2048), BF16)], axis=0)
+    for k in range(2):
+        upl[k] = lines[:, k * 1024 : (k + 1) * 1024]
 
     landed(wo, rsem.at[7], "wo")
     landed(frecv.at[pl.ds(0, 15)], rsem.at[9], "mixer")
     columns_out = [dot(mx[k].reshape(16, 1024), wo[k].reshape(128, 1024), 1, 1) for k in range(2)]
     osend[...] = (columns_out[0] + columns_out[1]).astype(BF16)
-    around(zc, 2 * NZ, lambda i: send(osend, orecv.at[zc], ssem.at[10], rsem.at[10], zc_dev(i)))
+    for k, e in zc_peers:
+        send(osend, orecv.at[zc], ssem.at[10], rsem.at[10], (k, y, x, e))
     orecv[zc] = osend[...]
     landed(tkz.at[pl.ds(0, NZ - 1)], rsem.at[11], "tkz")
     landed(orecv.at[pl.ds(0, 15)], rsem.at[10], "out")
@@ -284,9 +292,9 @@
     hidden = (tkz[...].reshape(16, 2048).astype(F32) + mixed).astype(BF16)
     hid[...] = hidden.reshape(NZ, 2, 2048)
     normed_mid = rms_scale(hidden.astype(F32), second_gain[...]).astype(BF16)
-    for k in range(2):
-        rows[k, mine8] = normed_mid[:, k * 1024 : (k + 1) * 1024].reshape(NZ, 2, 1024)
-    around(yx, NYX, lambda i: send(rows.at[c, mine8], rows.at[c, mine8], ssem.at[12], planesem.at[yx], yx_dev(i)))
+    rows[c, yx] = jnp.where(c == 0, normed_mid[:, 0:1024], normed_mid[:, 1024:2048])
+    for j, i in yx_peers:
+        send(rows.at[c, yx], rows.at[c, yx], ssem.at[12], planesem.at[yx], (z, j, i, c))
 
     driven = step_wide * conv_inner
     first_row = lax.broadcasted_iota(jnp.int32, (8, 512), 0) == 0
@@ -300,63 +308,79 @@
                 rate = jnp.broadcast_to(decay[s : s + 1, head : head + 1], (64, 128))
                 hs[s, head] = rate * hs[s, head] + update[h]
 
-    def forward(r, carry):
-        i = (yx + NYX - r) % NYX
-        block = rows.at[c, pl.ds(i * NZ, NZ)]
-        landed(block, planesem.at[i], "rows_yx")
-        send(block, block, ssem.at[13], rsem.at[13], partner)
-        return carry
-
-    lax.fori_loop(1, NYX, forward, 0)
-    copies[3].wait()
-    copies[4].wait()
-    copies[5].wait()
-
-    gate_line = dense_gate[...]
-    g_hi = gate_line.astype(BF16)
-    g_mid = (gate_line - g_hi.astype(F32)).astype(BF16)
-    g_lo = (gate_line - g_hi.astype(F32) - g_mid.astype(F32)).astype(BF16)
-    lines = jnp.concatenate([g_hi, g_mid, g_lo, jnp.zeros((5, 2048), BF16)], axis=0)
-    lines = jnp.stack([lines[:, 0:1024], lines[:, 1024:2048]])
-
-    def half_terms(k):
-        half = rows[k].reshape(256, 1024)
-        span = pl.ds(pl.multiple_of(k * 1024, 1024), 1024)
-        picked = dot(picks16, half).astype(BF16)
-        line = jnp.where(k == 0, lines[0], lines[1])
-        return (
-            dot(picked, eg[span]), dot(picked, eu[span]), dot(half, dense_up[:, span], 1, 1),
-            dot(half, line, 1, 1),
-        )
-
-    own_terms = half_terms(c)
-    landed(rows.at[other, pl.ds(0, 120)], rsem.at[13], "rows_d2d")
-    gate_pre, up_pre, pre, weigh = [a + b for a, b in zip(own_terms, half_terms(other))]
+    for i in (3, 4, 5):
+        copies[i].wait()
+
+    def use(k, j):
+        block = rows[k, pl.ds(j * NX, NX)].reshape(64, 1024)
+        span = pl.ds(pl.multiple_of(j * 64, 64), 64)
+        return dot(pt[span][:, 0:32], block, 0, 0), dot(block, upl[k], 1, 1)
+
+    def gather_of(j):
+        return pl.ds(j * NX, NX)
+
+    order = (0, 1, 3, 2)
+    picked_own, picked_other = None, None
+    pending = None
+
+    def take_other(j, total):
+        landed(rows.at[other, gather_of(j)], fsem.at[j], "rows_d2d")
+        got, pre = use(other, j)
+        pbuf[j] = pbuf[j] + pre
+        return got if total is None else total + got
+
+    for d in order:
+        j = y_at[d]
+        for e in (1, 3, 2) if d == 0 else (0, 1, 3, 2):
+            i = j * NX + x_at[e]
+            landed(rows.at[c, i], planesem.at[i], "rows_yx")
+        block = rows.at[c, gather_of(j)]
+        send(block, block, ssem.at[13], fsem.at[j], partner)
+        got, pre = use(c, j)
+        picked_own = got if picked_own is None else picked_own + got
+        pbuf[j] = pre
+        if pending is not None:
+            picked_other = take_other(pending, picked_other)
+        pending = j
+    picked_other = take_other(pending, picked_other)
+
+    pre = pbuf[...].reshape(256, 32)
+    weight = sigmoid(jnp.sum(pre[:, 16:19], axis=1, keepdims=True))
+    dense_act = silu(pre[:, 0:16]).astype(BF16).astype(F32) * weight
+    dact[...] = dense_act.astype(BF16)
+    send(dact, dactp, ssem.at[15], rsem.at[15], partner)
+    own16, other16 = picked_own.astype(BF16), picked_other.astype(BF16)
+    own_span = pl.ds(pl.multiple_of(c * 1024, 1024), 1024)
+    other_span = pl.ds(pl.multiple_of(other * 1024, 1024), 1024)
+    gate_pre = dot(own16, eg[own_span]) + dot(other16, eg[other_span])
+    up_pre = dot(own16, eu[own_span]) + dot(other16, eu[other_span])
     glu_part = jnp.minimum(gate_pre, clamp_limit)
     lin_part = jnp.clip(up_pre, -clamp_limit, clamp_limit)
     activated = (glu_part * sigmoid(glu_alpha * glu_part) * (lin_part + 1.0)).astype(BF16)
-    part = dot(activated, ed[...]) * slot_weight
-    epart[...] = jnp.where(c == 0, part[:, 1024:2048], part[:, 0:1024]).astype(BF16)
+    epart[...] = (dot(activated, ed[:, other_span]) * slot_weight).astype(BF16)
     send(epart, epartp, ssem.at[14], rsem.at[14], partner)
-    own_part = jnp.where(c == 0, part[:, 0:1024], part[:, 1024:2048])
-    weight = sigmoid(jnp.sum(weigh, axis=1, keepdims=True))
-    dense_act = silu(pre).astype(BF16).astype(F32) * weight
-    dact[...] = dense_act.astype(BF16)
-    send(dact, dactp, ssem.at[15], rsem.at[15], partner)
+    own_part = dot(activated, ed[:, own_span]) * slot_weight
     landed(ddp, rsem.at[8], "ddp")
+    landed(dactp, rsem.at[15], "dact")
+    down = jnp.concatenate([dense_down[:, own_span], ddp[...]], axis=0)
+    dense_term = dot(jnp.concatenate([dact[...], dactp[...]], axis=1), down)
     landed(epartp, rsem.at[14], "epart")
     both = (own_part + epartp[...].astype(F32)).astype(BF16)
-    landed(dactp, rsem.at[15], "dact")
-    left = jnp.concatenate([dact[...], dactp[...], picks_t[:, 0:32].astype(BF16)], axis=1)
-    own_down = jnp.where(c == 0, dense_down[:, 0:1024], dense_down[:, 1024:2048])
-    right = jnp.concatenate([own_down, ddp[...], both], axis=0)
-    tsum.reshape(256, 1024)[...] = dot(left, right).astype(BF16)
-
-    around(yx, NYX, lambda i: send(tsum.at[pl.ds(i * NZ, NZ)], prs.at[yx], ssem.at[16], rsem.at[16], yx_dev(i)))
-    prs[yx] = tsum[mine8]
+
+    dterm[...] = dense_term.reshape(NY, 64, 1024)
+    for d in (2, 1, 3, 0):
+        j = y_at[d]
+        span = pl.ds(pl.multiple_of(j * 64, 64), 64)
+        total = dterm[j] + dot(pt[span][:, 0:32], both)
+        tsum[gather_of(j)] = total.astype(BF16).reshape(NX, 16, 1024)
+        for e in (2, 1, 3) if d == 0 else (2, 1, 3, 0):
+            i = x_at[e]
+            send(tsum.at[j * NX + i], prs.at[yx], ssem.at[16], rsem.at[16], (z, j, i, c))
+    prs[yx] = tsum[yx]
     landed(prs.at[pl.ds(0, NYX - 1)], rsem.at[16], "sum_yx")
-    fsend[...] = jnp.sum(prs[...].astype(F32), axis=0).astype(BF16)
-    around(zc, 2 * NZ, lambda i: send(fsend.at[i // 2], frecv.at[zc], ssem.at[17], rsem.at[17], zc_dev(i)))
+    fsend[...] = jnp.sum(prs[...].astype(F32), axis=0).astype(BF16).reshape(NZ, 2, 1024)
+    for k, e in zc_peers:
+        send(fsend.at[k], frecv.at[zc], ssem.at[17], rsem.at[17], (k, y, x, e))
     frecv[zc] = fsend[z]
     landed(frecv.at[pl.ds(0, 15)], rsem.at[17], "sum_z")
     final = []
@@ -372,8 +396,8 @@
         tok.at[pl.ds(0, NZY - 1)], wi.at[pl.ds(0, NX - 1)], wg.at[pl.ds(0, NX - 1)],
         rts.at[pl.ds(0, NZ - 1)], psend_i.at[pl.ds(0, NZY - 1)], psend_g.at[pl.ds(0, NZY - 1)],
         rts.at[pl.ds(0, 120)], None, ddp, frecv.at[pl.ds(0, 15)],
-        orecv.at[pl.ds(0, 15)], tkz.at[pl.ds(0, NZ - 1)], rows.at[0, pl.ds(0, 120)],
-        rows.at[0, pl.ds(0, 120)],
+        orecv.at[pl.ds(0, 15)], tkz.at[pl.ds(0, NZ - 1)], rows.at[0, pl.ds(0, NYX - 1)],
+        rows.at[0],
         epart, dact, prs.at[pl.ds(0, NYX - 1)], frecv.at[pl.ds(0, 15)],
     )):
         if ref is not None:
@@ -386,6 +410,15 @@
     @pl.when(keeper != c)
     def _():
         landed(wo, ssem.at[7])
+
+
+def write_kernel(*refs):
+    sems = refs[8]
+    copies = [pltpu.make_async_copy(refs[i], refs[4 + i], sems.at[i]) for i in range(4)]
+    for i in (3, 0, 1, 2):
+        copies[i].start()
+    for copy in copies:
+        copy.wait()
 
 
 def local(
@@ -413,7 +446,7 @@
         jax.ShapeDtypeStruct((2, 3, 2, 256), BF16),
         jax.ShapeDtypeStruct((2, 16, 64, 128), F32),
     )
-    layer_out, conv_out, conv_proj_out, state_out = pl.pallas_call(
+    results = pl.pallas_call(
         layer_kernel,
         out_shape=tuple(V(o.shape, o.dtype) for o in outs),
         in_specs=[anywhere] * (len(near) + len(far)),
@@ -428,12 +461,13 @@
             V((NZY, 2, 1024), BF16), V((NZY, 2, 1024), BF16),
             V((128, 2, 256), BF16), V((2, 8, 16, 1024), BF16), V((2, NZ, 2, 1024), BF16),
             V((16, 128), BF16), V((2 * NZ, 16, 128), BF16), V((NZ, 2, 2048), BF16), V((NZ, 2, 2048), BF16),
-            V((2, 128, 2, 1024), BF16), V((16, 1024), BF16), V((256, 16), BF16), V((256, 16), BF16),
+            V((2, NYX, 16, 1024), BF16), V((16, 1024), BF16), V((256, 16), BF16), V((256, 16), BF16),
             V((32, 1024), BF16), V((32, 1024), BF16),
-            V((128, 2, 1024), BF16), V((NYX, NZ, 2, 1024), BF16), V((NZ, 2, 1024), BF16),
-            V((2 * NZ, 2, 1024), BF16),
+            V((NYX, 16, 1024), BF16), V((NYX, 16, 1024), BF16), V((NZ, 2, 1024), BF16),
+            V((2 * NZ, 2, 1024), BF16), V((256, 128), BF16), V((2, 32, 1024), BF16),
+            V((NY, 64, 32), F32), V((NY, 64, 1024), F32),
             pltpu.SemaphoreType.DMA((NEAR,)), pltpu.SemaphoreType.DMA((8,)), pltpu.SemaphoreType.DMA((18,)),
-            pltpu.SemaphoreType.DMA((18,)), pltpu.SemaphoreType.DMA((NYX,)),
+            pltpu.SemaphoreType.DMA((18,)), pltpu.SemaphoreType.DMA((NYX,)), pltpu.SemaphoreType.DMA((NY,)),
         ],
         compiler_params=pltpu.CompilerParams(
             collective_id=0, has_side_effects=True, vmem_limit_bytes=56 * 1024 * 1024
@@ -441,6 +475,15 @@
         cost_estimate=pl.CostEstimate(flops=2 * 10**9, bytes_accessed=16 * 2**20, transcendentals=10**5),
         name="layer",
     )(*near, *far)
+    results = [pltpu.with_memory_space_constraint(r, V) for r in results]
+    layer_out, conv_out, conv_proj_out, state_out = pl.pallas_call(
+        write_kernel,
+        out_shape=outs,
+        in_specs=[vmem] * 4,
+        out_specs=[anywhere] * 4,
+        scratch_shapes=[pltpu.SemaphoreType.DMA((4,))],
+        name="write",
+    )(*results)
     return (layer_out, state_out, conv_out.transpose(1, 0, 2), conv_proj_out)
 
 

time: 69.9 us -> 65 us (0.930)
  local copies, waits for them, and re-layouts: 2.76 us -> 0 us
  Pallas kernels: 66.4 us -> 64.2 us
    pallas_call x1, Pallas kernels: 66.4 us -> 63.2 us  [local(): pl.pallas_call(layer_kernel, out_shape=tuple((V(o.shape, o.dtype) for o i...]
    unnamed x4 -> x0, local copies, waits for them, and re-layouts: 2.76 us -> none
    pallas_call x0 -> x1, Pallas kernels: none -> 1.01 us  [local(): pl.pallas_call(write_kernel, out_shape=outs, in_specs=[vmem] * 4, out_spe...]
where the time goes in v3:
time: 65 us; the launch traced here: 64.9 us
  Pallas kernels  64.2 us (99%)
  between operations  0.65 us (1%)
    pallas_call x1, Pallas kernels, local(): pl.pallas_call(layer_kernel, out_shape=tuple((V(o.shape, o.dtype) for o i...  63.2 us

profile of v3, /device:TPU:1, one launch (start us, length us, event | category | flops | bytes accessed | tf_op | source)
XLA Modules:
  0.0 64.9 jit_solution(16432195621752966311)
XLA Ops:
  0.6 63.2 %layer.1 = (bf16[1,2048]{1,0:T(2,128)(2,1)S(1)}, bf16[3,2,1024]{2,1,0:T(2,128)(2,1)S(1)}, bf16[2,3,2,256]{3,2,1,0:T(2,128)(2,1)S(1)}, f32[2,16,64,128]{3,2,1,0:T(8,128)S(1)}) custom-call(bf16[2,2048]{1,0:T(2,128)(2,1)} %refs_0_.1, f32[1,2048]{1,0:T(1,128)} %bitcast.16, bf16[16,2048]{1,0:T(8,128)(2,1)} %bitcast.12, bf16[3,2,1024]{2,1,0:T(2,128)(2,1)} %bitcast.15, ...), custom_call_target="tpu_custom_call" | custom-call | flops 2000000000 | bytes 16777216 | tf_op jit(solution)/shard_map/layer/pallas_call | solution.py:449
  63.9 1.0 %write.1 = (bf16[1,2048]{1,0:T(2,128)(2,1)}, bf16[3,2,1024]{2,1,0:T(2,128)(2,1)}, bf16[2,3,2,256]{3,2,1,0:T(2,128)(2,1)}, f32[2,16,64,128]{3,2,1,0:T(8,128)}) custom-call(bf16[1,2048]{1,0:T(2,128)(2,1)S(1)} %get-tuple-element.12.refs_0_, bf16[3,2,1024]{2,1,0:T(2,128)(2,1)S(1)} %get-tuple-element.13.refs_1_, ...), custom_call_target="tpu_custom_call" | custom-call | tf_op jit(solution)/shard_map/write/pallas_call | solution.py:479

commit v4 on v3

--- a/solution.py
+++ b/solution.py
@@ -19,6 +19,7 @@
 highest = lax.Precision.HIGHEST
 NZ, NY, NX = 8, 4, 4
 NZY, NYX = NZ * NY, NY * NX
+WIDE = 768
 
 
 sigmoid = jax.nn.sigmoid
@@ -57,7 +58,8 @@
     (
         ww, rw, eg, eu, ed, wg, wi, nblk, tok, psend_i, psend_g, precv_i, precv_g, rts, wo, mx,
         osend, orecv, tkz, hid, rows, ddp, dact, dactp, epart, epartp, tsum, prs, fsend, frecv,
-        pt, upl, pbuf, dterm, nsem, lsem, ssem, rsem, planesem, fsem,
+        pt, upl, upp, pbuf, pmsg, pgot, pickm, pickp, dterm, perm, pz, zsum,
+        zrs, zsend, zrecv, lsem, ssem, rsem, planesem,
     ) = refs
     z, y, x, c = [lax.axis_index(n) for n in EP_TP]
     zy = z * NY + y
@@ -100,17 +102,15 @@
     for k in z_peers:
         hello((k, y, x, other))
 
-    small = [pltpu.make_async_copy(a, b, nsem.at[i]) for i, (a, b) in enumerate(zip(near_hbm, near))]
+    small = [pltpu.make_async_copy(a, b, ssem.at[i]) for i, (a, b) in enumerate(zip(near_hbm, near))]
     loads = [
         (write_weight, ww), (read_weight, rw), (head_state, hs), (expert_gate.at[0], eg),
         (expert_up.at[0], eu), (expert_down.at[0], ed), (gate_weight, wg.at[x]),
         (inner_weight, wi.at[x]),
     ]
     copies = [pltpu.make_async_copy(a, b, lsem.at[i]) for i, (a, b) in enumerate(loads)]
-    for copy in small:
+    for copy in [*small, copies[7], copies[6]]:
         copy.start()
-    for i in (7, 6, 0, 1, 2, 3, 4, 5):
-        copies[i].start()
     small[0].wait()
     small[1].wait()
 
@@ -119,8 +119,9 @@
         nblk[b] = normed[:, b * 128 : (b + 1) * 128]
     tok[zy] = nblk[zy // 2]
     tkz[z] = tokens[...]
-    small[12].wait()
-    small[13].wait()
+    with jax.named_scope("small"):
+        for copy in [*small[2:], copies[7], copies[6]]:
+            copy.wait()
     blank = jnp.zeros((2, 124), F32)
     rts[base + z] = jnp.concatenate(
         [routes[...].astype(F32), blank, route_logits[...].astype(F32), blank], axis=1
@@ -134,9 +135,9 @@
     for k in z_peers:
         send(rts.at[base + z], rts.at[base + z], ssem.at[3], rsem.at[3], (k, y, x, c))
     for i in (x_at[2], x_at[1], x_at[3]):
-        send(inner_weight, wi.at[x], ssem.at[1], rsem.at[1], (z, y, i, c))
+        send(wi.at[x], wi.at[x], ssem.at[1], rsem.at[1], (z, y, i, c))
     for i in (x_at[2], x_at[1], x_at[3]):
-        send(gate_weight, wg.at[x], ssem.at[2], rsem.at[2], (z, y, i, c))
+        send(wg.at[x], wg.at[x], ssem.at[2], rsem.at[2], (z, y, i, c))
     for k in z_peers:
         send(tkz.at[z], tkz.at[z], ssem.at[11], rsem.at[11], (k, y, x, c))
     keeper = yx // 8
@@ -153,9 +154,9 @@
     def _():
         send(out_weight, place, ssem.at[7], rsem.at[7], partner)
 
-    for copy in small[2:12] + small[14:]:
-        copy.wait()
-
+
+    for i in (0, 1, 2, 3, 4, 5):
+        copies[i].start()
     with jax.named_scope("ww"):
         copies[0].wait()
         copies[1].wait()
@@ -163,8 +164,6 @@
     read_proj = dot(normed, rw[...]).astype(BF16)
     step_raw = dot(normed, step_weight[...], 1, 1)
 
-    copies[6].wait()
-    copies[7].wait()
     landed(tok.at[pl.ds(0, NZY - 1)], rsem.at[0], "tok")
     landed(rts.at[pl.ds(0, NZ - 1)], rsem.at[3], "rt_z")
     mine8 = pl.ds(base, NZ)
@@ -187,7 +186,10 @@
     for k, j in zy_peers:
         send(psend_g.at[k * NY + j], precv_g.at[zy], ssem.at[5], rsem.at[5], (k, j, x, c))
     precv_g[zy] = psend_g[zy]
-    send(dense_down.at[:, pl.ds(pl.multiple_of(other * 1024, 1024), 1024)], ddp, ssem.at[8], rsem.at[8], partner)
+    own_span = pl.ds(pl.multiple_of(c * 1024, 1024), 1024)
+    other_span = pl.ds(pl.multiple_of(other * 1024, 1024), 1024)
+    send(dense_down.at[:, other_span], ddp, ssem.at[8], rsem.at[8], partner)
+    send(dense_up.at[:, other_span], upp, ssem.at[19], rsem.at[12], partner)
 
     cps = conv_proj_state[...].astype(F32)
     cpk = conv_proj_kernel[...]
@@ -271,16 +273,21 @@
     picks_t = jnp.where((count_col - 1.0 == lane.astype(F32)) & (chosen > 0.5), 1.0, 0.0)
     slot_weight = dot(picks, jnp.broadcast_to(row_weight, (256, 128)), precision=highest)[:, 0:1]
     pt[...] = picks_t.astype(BF16)
+    turned = ((cc >> 1) & 15) * 16 + (cc >> 5) * 2 + (cc & 1)
+    perm[...] = (rr == turned).astype(BF16)
+    pz[...] = dot(picks.astype(BF16), perm[...]).astype(BF16)
     gate_line = dense_gate[...]
     g_hi = gate_line.astype(BF16)
     g_mid = (gate_line - g_hi.astype(F32)).astype(BF16)
     g_lo = (gate_line - g_hi.astype(F32) - g_mid.astype(F32)).astype(BF16)
-    lines = jnp.concatenate([dense_up[...], g_hi, g_mid, g_lo, jnp.zeros((13, 2048), BF16)], axis=0)
-    for k in range(2):
-        upl[k] = lines[:, k * 1024 : (k + 1) * 1024]
+    lines = jnp.concatenate([g_hi, g_mid, g_lo, jnp.zeros((13, 2048), BF16)], axis=0)
+    upl[0:16] = dense_up[:, own_span]
+    upl[16:32] = jnp.where(c == 0, lines[:, 0:1024], lines[:, 1024:2048])
+    landed(upp, rsem.at[12], "upp")
+    upl[32:48] = upp[...]
 
     landed(wo, rsem.at[7], "wo")
-    landed(frecv.at[pl.ds(0, 15)], rsem.at[9], "mixer")
+    landed(precv_i.at[pl.ds(0, 15)], rsem.at[9], "mixer")
     columns_out = [dot(mx[k].reshape(16, 1024), wo[k].reshape(128, 1024), 1, 1) for k in range(2)]
     osend[...] = (columns_out[0] + columns_out[1]).astype(BF16)
     for k, e in zc_peers:
@@ -294,7 +301,7 @@
     normed_mid = rms_scale(hidden.astype(F32), second_gain[...]).astype(BF16)
     rows[c, yx] = jnp.where(c == 0, normed_mid[:, 0:1024], normed_mid[:, 1024:2048])
     for j, i in yx_peers:
-        send(rows.at[c, yx], rows.at[c, yx], ssem.at[12], planesem.at[yx], (z, j, i, c))
+        send(rows.at[c, yx], rows.at[c, yx], ssem.at[12], planesem.at[y], (z, j, i, c))
 
     driven = step_wide * conv_inner
     first_row = lax.broadcasted_iota(jnp.int32, (8, 512), 0) == 0
@@ -311,49 +318,31 @@
     for i in (3, 4, 5):
         copies[i].wait()
 
-    def use(k, j):
-        block = rows[k, pl.ds(j * NX, NX)].reshape(64, 1024)
-        span = pl.ds(pl.multiple_of(j * 64, 64), 64)
-        return dot(pt[span][:, 0:32], block, 0, 0), dot(block, upl[k], 1, 1)
-
-    def gather_of(j):
-        return pl.ds(j * NX, NX)
-
-    order = (0, 1, 3, 2)
-    picked_own, picked_other = None, None
-    pending = None
-
-    def take_other(j, total):
-        landed(rows.at[other, gather_of(j)], fsem.at[j], "rows_d2d")
-        got, pre = use(other, j)
-        pbuf[j] = pbuf[j] + pre
-        return got if total is None else total + got
-
-    for d in order:
+    picked = None
+    for d in (0, 1, 3, 2):
         j = y_at[d]
-        for e in (1, 3, 2) if d == 0 else (0, 1, 3, 2):
-            i = j * NX + x_at[e]
-            landed(rows.at[c, i], planesem.at[i], "rows_yx")
-        block = rows.at[c, gather_of(j)]
-        send(block, block, ssem.at[13], fsem.at[j], partner)
-        got, pre = use(c, j)
-        picked_own = got if picked_own is None else picked_own + got
-        pbuf[j] = pre
-        if pending is not None:
-            picked_other = take_other(pending, picked_other)
-        pending = j
-    picked_other = take_other(pending, picked_other)
-
-    pre = pbuf[...].reshape(256, 32)
-    weight = sigmoid(jnp.sum(pre[:, 16:19], axis=1, keepdims=True))
-    dense_act = silu(pre[:, 0:16]).astype(BF16).astype(F32) * weight
-    dact[...] = dense_act.astype(BF16)
+        landed(rows.at[c, pl.ds(0, 3 if d == 0 else 4)], planesem.at[j], "rows_yx")
+        block = rows[c, pl.ds(pl.multiple_of(j * NX, NX), NX)].reshape(64, 1024)
+        got = dot(pt[pl.ds(pl.multiple_of(j * 64, 64), 64)][:, 0:32], block, 0, 0)
+        picked = got if picked is None else picked + got
+        if d == 2:
+            pickm[...] = picked.astype(BF16)
+            send(pickm, pickp, ssem.at[13], rsem.at[13], partner)
+        pbuf[j] = dot(upl[...], block, 1, 1)
+    sums = jnp.concatenate([pbuf[j] for j in range(NY)], axis=1)
+    pmsg[...] = jnp.concatenate([sums[32:48], sums[16:32]], axis=0)
+    send(pmsg, pgot, ssem.at[18], rsem.at[18], partner)
+    own16 = picked.astype(BF16)
+    gate_pre = dot(own16, eg[own_span])
+    up_pre = dot(own16, eu[own_span])
+    landed(pgot, rsem.at[18], "pgot")
+    pre = sums[0:32] + pgot[...]
+    weight = sigmoid(jnp.sum(pre[16:19], axis=0, keepdims=True))
+    dact[...] = (silu(pre[0:16]).astype(BF16).astype(F32) * weight).astype(BF16)
     send(dact, dactp, ssem.at[15], rsem.at[15], partner)
-    own16, other16 = picked_own.astype(BF16), picked_other.astype(BF16)
-    own_span = pl.ds(pl.multiple_of(c * 1024, 1024), 1024)
-    other_span = pl.ds(pl.multiple_of(other * 1024, 1024), 1024)
-    gate_pre = dot(own16, eg[own_span]) + dot(other16, eg[other_span])
-    up_pre = dot(own16, eu[own_span]) + dot(other16, eu[other_span])
+    landed(pickp, rsem.at[13], "pickp")
+    gate_pre = gate_pre + dot(pickp[...], eg[other_span])
+    up_pre = up_pre + dot(pickp[...], eu[other_span])
     glu_part = jnp.minimum(gate_pre, clamp_limit)
     lin_part = jnp.clip(up_pre, -clamp_limit, clamp_limit)
     activated = (glu_part * sigmoid(glu_alpha * glu_part) * (lin_part + 1.0)).astype(BF16)
@@ -363,49 +352,67 @@
     landed(ddp, rsem.at[8], "ddp")
     landed(dactp, rsem.at[15], "dact")
     down = jnp.concatenate([dense_down[:, own_span], ddp[...]], axis=0)
-    dense_term = dot(jnp.concatenate([dact[...], dactp[...]], axis=1), down)
+    dense_both = jnp.concatenate([dact[...], dactp[...]], axis=0)
+    dterm[...] = dot(dense_both, down[:, 0:WIDE], 0, 0).reshape(NY, 64, WIDE)
+    dense_turned = dot(dense_both, perm[...]).astype(BF16)
     landed(epartp, rsem.at[14], "epart")
     both = (own_part + epartp[...].astype(F32)).astype(BF16)
 
-    dterm[...] = dense_term.reshape(NY, 64, 1024)
+    first_z = dot(
+        jnp.concatenate([dense_turned, pz[...]], axis=0),
+        jnp.concatenate([down[:, WIDE:], both[:, WIDE:]], axis=0), 0, 0,
+    )
+    zsum[...] = first_z.astype(BF16).reshape(NZ, 32, 1024 - WIDE)
+    for k in z_peers:
+        send(zsum.at[k], zrs.at[z], ssem.at[20], rsem.at[16], (k, y, x, c))
+    zrs[z] = zsum[z]
     for d in (2, 1, 3, 0):
         j = y_at[d]
         span = pl.ds(pl.multiple_of(j * 64, 64), 64)
-        total = dterm[j] + dot(pt[span][:, 0:32], both)
-        tsum[gather_of(j)] = total.astype(BF16).reshape(NX, 16, 1024)
+        total = dterm[j] + dot(pt[span][:, 0:32], both[:, 0:WIDE])
+        tsum[pl.ds(pl.multiple_of(j * NX, NX), NX)] = total.astype(BF16).reshape(NX, 16, WIDE)
         for e in (2, 1, 3) if d == 0 else (2, 1, 3, 0):
             i = x_at[e]
-            send(tsum.at[j * NX + i], prs.at[yx], ssem.at[16], rsem.at[16], (z, j, i, c))
+            send(tsum.at[j * NX + i], prs.at[yx], ssem.at[16], rsem.at[19], (z, j, i, c))
     prs[yx] = tsum[yx]
-    landed(prs.at[pl.ds(0, NYX - 1)], rsem.at[16], "sum_yx")
-    fsend[...] = jnp.sum(prs[...].astype(F32), axis=0).astype(BF16).reshape(NZ, 2, 1024)
+    landed(zrs.at[pl.ds(0, NZ - 1)], rsem.at[16], "sum_z1")
+    zsend[...] = jnp.sum(zrs[...].astype(F32), axis=0).astype(BF16).reshape(NYX, 2, 1024 - WIDE)
+    for j, i in yx_peers:
+        for e in c_at:
+            send(zsend.at[j * NX + i], zrecv.at[yx * 2 + c], ssem.at[21], rsem.at[20], (z, j, i, e))
+    send(zsend.at[yx], zrecv.at[yx * 2 + c], ssem.at[21], rsem.at[20], partner)
+    zrecv[yx * 2 + c] = zsend[yx]
+    landed(prs.at[pl.ds(0, NYX - 1)], rsem.at[19], "sum_yx")
+    fsend[...] = jnp.sum(prs[...].astype(F32), axis=0).astype(BF16).reshape(NZ, 2, WIDE)
     for k, e in zc_peers:
         send(fsend.at[k], frecv.at[zc], ssem.at[17], rsem.at[17], (k, y, x, e))
     frecv[zc] = fsend[z]
+    landed(zrecv.at[pl.ds(0, 31)], rsem.at[20], "sum_yx2")
+    narrow = [sum(zrecv[2 * i + k].astype(F32) for i in range(NYX)) for k in range(2)]
     landed(frecv.at[pl.ds(0, 15)], rsem.at[17], "sum_z")
     final = []
     for k in range(2):
         total = frecv[k].astype(F32)
         for i in range(1, NZ):
             total = total + frecv[2 * i + k].astype(F32)
-        final.append(total)
+        final += [total, narrow[k]]
     result = hid[z].astype(F32) + jnp.concatenate(final, axis=1)
     layer_out[...] = jnp.where(c == 0, result[0:1], result[1:2]).astype(BF16)
 
     for i, ref in enumerate((
         tok.at[pl.ds(0, NZY - 1)], wi.at[pl.ds(0, NX - 1)], wg.at[pl.ds(0, NX - 1)],
         rts.at[pl.ds(0, NZ - 1)], psend_i.at[pl.ds(0, NZY - 1)], psend_g.at[pl.ds(0, NZY - 1)],
-        rts.at[pl.ds(0, 120)], None, ddp, frecv.at[pl.ds(0, 15)],
+        rts.at[pl.ds(0, 120)], None, ddp, precv_i.at[pl.ds(0, 15)],
         orecv.at[pl.ds(0, 15)], tkz.at[pl.ds(0, NZ - 1)], rows.at[0, pl.ds(0, NYX - 1)],
-        rows.at[0],
-        epart, dact, prs.at[pl.ds(0, NYX - 1)], frecv.at[pl.ds(0, 15)],
+        pickm, epart, dact, prs.at[pl.ds(0, NYX - 1)], frecv.at[pl.ds(0, 15)], pmsg, upp,
+        zrs.at[pl.ds(0, NZ - 1)], zrecv.at[pl.ds(0, 31)],
     )):
         if ref is not None:
             landed(ref, ssem.at[i])
 
     @pl.when(keeper == c)
     def _():
-        landed(prs.at[pl.ds(0, NYX - 1)], ssem.at[7])
+        landed(rows.at[0, pl.ds(0, NYX - 1)], ssem.at[7])
 
     @pl.when(keeper != c)
     def _():
@@ -461,13 +468,17 @@
             V((NZY, 2, 1024), BF16), V((NZY, 2, 1024), BF16),
             V((128, 2, 256), BF16), V((2, 8, 16, 1024), BF16), V((2, NZ, 2, 1024), BF16),
             V((16, 128), BF16), V((2 * NZ, 16, 128), BF16), V((NZ, 2, 2048), BF16), V((NZ, 2, 2048), BF16),
-            V((2, NYX, 16, 1024), BF16), V((16, 1024), BF16), V((256, 16), BF16), V((256, 16), BF16),
+            V((2, NYX, 16, 1024), BF16), V((16, 1024), BF16), V((16, 256), BF16), V((16, 256), BF16),
             V((32, 1024), BF16), V((32, 1024), BF16),
-            V((NYX, 16, 1024), BF16), V((NYX, 16, 1024), BF16), V((NZ, 2, 1024), BF16),
-            V((2 * NZ, 2, 1024), BF16), V((256, 128), BF16), V((2, 32, 1024), BF16),
-            V((NY, 64, 32), F32), V((NY, 64, 1024), F32),
-            pltpu.SemaphoreType.DMA((NEAR,)), pltpu.SemaphoreType.DMA((8,)), pltpu.SemaphoreType.DMA((18,)),
-            pltpu.SemaphoreType.DMA((18,)), pltpu.SemaphoreType.DMA((NYX,)), pltpu.SemaphoreType.DMA((NY,)),
+            V((NYX, 16, WIDE), BF16), V((NYX, 16, WIDE), BF16), V((NZ, 2, WIDE), BF16),
+            V((2 * NZ, 2, WIDE), BF16), V((256, 128), BF16), V((48, 1024), BF16),
+            V((16, 1024), BF16), V((NY, 48, 64), F32), V((32, 256), F32), V((32, 256), F32),
+            V((32, 1024), BF16), V((32, 1024), BF16), V((NY, 64, WIDE), F32),
+            V((256, 256), BF16), V((32, 256), BF16), V((NZ, 32, 1024 - WIDE), BF16),
+            V((NZ, 32, 1024 - WIDE), BF16), V((NYX, 2, 1024 - WIDE), BF16),
+            V((2 * NYX, 2, 1024 - WIDE), BF16),
+            pltpu.SemaphoreType.DMA((8,)), pltpu.SemaphoreType.DMA((22,)),
+            pltpu.SemaphoreType.DMA((21,)), pltpu.SemaphoreType.DMA((NY,)),
         ],
         compiler_params=pltpu.CompilerParams(
             collective_id=0, has_side_effects=True, vmem_limit_bytes=56 * 1024 * 1024

time: 65 us -> 61.9 us (0.952)
  Pallas kernels: 64.2 us -> 61.1 us
    pallas_call x1, Pallas kernels: 63.2 us -> 60.1 us  [local(): pl.pallas_call(layer_kernel, out_shape=tuple((V(o.shape, o.dtype) for o i...]
where the time goes in v4:
time: 61.9 us; the launch traced here: 61.8 us
  Pallas kernels  61.1 us (99%)
  between operations  0.65 us (1%)
    pallas_call x1, Pallas kernels, local(): pl.pallas_call(layer_kernel, out_shape=tuple((V(o.shape, o.dtype) for o i...  60.1 us

profile of v4, /device:TPU:1, one launch (start us, length us, event | category | flops | bytes accessed | tf_op | source)
XLA Modules:
  0.0 61.8 jit_solution(15579641265425460599)
XLA Ops:
  0.6 60.1 %layer.1 = (bf16[1,2048]{1,0:T(2,128)(2,1)S(1)}, bf16[3,2,1024]{2,1,0:T(2,128)(2,1)S(1)}, bf16[2,3,2,256]{3,2,1,0:T(2,128)(2,1)S(1)}, f32[2,16,64,128]{3,2,1,0:T(8,128)S(1)}) custom-call(bf16[2,2048]{1,0:T(2,128)(2,1)} %refs_0_.1, f32[1,2048]{1,0:T(1,128)} %bitcast.16, bf16[16,2048]{1,0:T(8,128)(2,1)} %bitcast.12, bf16[3,2,1024]{2,1,0:T(2,128)(2,1)} %bitcast.15, ...), custom_call_target="tpu_custom_call" | custom-call | flops 2000000000 | bytes 16777216 | tf_op jit(solution)/shard_map/layer/pallas_call | solution.py:456
  60.7 1.0 %write.1 = (bf16[1,2048]{1,0:T(2,128)(2,1)}, bf16[3,2,1024]{2,1,0:T(2,128)(2,1)}, bf16[2,3,2,256]{3,2,1,0:T(2,128)(2,1)}, f32[2,16,64,128]{3,2,1,0:T(8,128)}) custom-call(bf16[1,2048]{1,0:T(2,128)(2,1)S(1)} %get-tuple-element.12.refs_0_, bf16[3,2,1024]{2,1,0:T(2,128)(2,1)S(1)} %get-tuple-element.13.refs_1_, ...), custom_call_target="tpu_custom_call" | custom-call | tf_op jit(solution)/shard_map/write/pallas_call | solution.py:490

commit v5 on v4

--- a/solution.py
+++ b/solution.py
@@ -57,9 +57,9 @@
     ) = near
     (
         ww, rw, eg, eu, ed, wg, wi, nblk, tok, psend_i, psend_g, precv_i, precv_g, rts, wo, mx,
-        osend, orecv, tkz, hid, rows, ddp, dact, dactp, epart, epartp, tsum, prs, fsend, frecv,
+        osend, orecv, tkz, hown, hgot, rows, ddp, dact, dactp, epart, epartp, tsum, prs, fsend, frecv,
         pt, upl, upp, pbuf, pmsg, pgot, pickm, pickp, dterm, perm, pz, zsum,
-        zrs, zsend, zrecv, lsem, ssem, rsem, planesem,
+        zrs, zsend, zrecv, pk, lsem, ssem, rsem, planesem, osem,
     ) = refs
     z, y, x, c = [lax.axis_index(n) for n in EP_TP]
     zy = z * NY + y
@@ -273,6 +273,7 @@
     picks_t = jnp.where((count_col - 1.0 == lane.astype(F32)) & (chosen > 0.5), 1.0, 0.0)
     slot_weight = dot(picks, jnp.broadcast_to(row_weight, (256, 128)), precision=highest)[:, 0:1]
     pt[...] = picks_t.astype(BF16)
+    pk[...] = picks
     turned = ((cc >> 1) & 15) * 16 + (cc >> 5) * 2 + (cc & 1)
     perm[...] = (rr == turned).astype(BF16)
     pz[...] = dot(picks.astype(BF16), perm[...]).astype(BF16)
@@ -289,19 +290,46 @@
     landed(wo, rsem.at[7], "wo")
     landed(precv_i.at[pl.ds(0, 15)], rsem.at[9], "mixer")
     columns_out = [dot(mx[k].reshape(16, 1024), wo[k].reshape(128, 1024), 1, 1) for k in range(2)]
-    osend[...] = (columns_out[0] + columns_out[1]).astype(BF16)
-    for k, e in zc_peers:
-        send(osend, orecv.at[zc], ssem.at[10], rsem.at[10], (k, y, x, e))
-    orecv[zc] = osend[...]
     landed(tkz.at[pl.ds(0, NZ - 1)], rsem.at[11], "tkz")
-    landed(orecv.at[pl.ds(0, 15)], rsem.at[10], "out")
-    mixed = jnp.concatenate([orecv[k].astype(F32) for k in range(2 * NZ)], axis=1)
-    hidden = (tkz[...].reshape(16, 2048).astype(F32) + mixed).astype(BF16)
-    hid[...] = hidden.reshape(NZ, 2, 2048)
-    normed_mid = rms_scale(hidden.astype(F32), second_gain[...]).astype(BF16)
-    rows[c, yx] = jnp.where(c == 0, normed_mid[:, 0:1024], normed_mid[:, 1024:2048])
-    for j, i in yx_peers:
-        send(rows.at[c, yx], rows.at[c, yx], ssem.at[12], planesem.at[y], (z, j, i, c))
+    mine128 = tkz[:, :, pl.ds(pl.multiple_of(zc * 128, 128), 128)].reshape(16, 128)
+    osend[...] = (mine128.astype(F32) + columns_out[0] + columns_out[1]).astype(BF16)
+    holder = z // 4
+    place8 = (z % 4) * 2 + c
+    third = (z % 4) // 2
+    for k in z_peers:
+        send(osend, orecv.at[place8], ssem.at[10], osem.at[third], (k, y, x, holder))
+
+    @pl.when(holder != c)
+    def _():
+        send(osend, orecv.at[place8], ssem.at[10], osem.at[third], partner)
+
+    @pl.when(holder == c)
+    def _():
+        orecv[place8] = osend[...]
+
+    near_group = third + (1 - 2 * third) * (holder + c - 2 * holder * c)
+    own_rows = []
+    for n in range(2):
+        q = near_group + n * (1 - 2 * near_group)
+        if n == 0:
+
+            @pl.when(holder == c)
+            def _():
+                landed(orecv.at[pl.ds(0, 3)], osem.at[q], "out")
+
+            @pl.when(holder != c)
+            def _():
+                landed(orecv.at[pl.ds(0, 4)], osem.at[q], "out")
+        else:
+            landed(orecv.at[pl.ds(0, 4)], osem.at[q], "out2")
+        for i in range(4):
+            rows[q, yx, :, i * 128 : (i + 1) * 128] = orecv[q * 4 + i]
+        for j, i in yx_peers:
+            send(rows.at[q, yx], rows.at[q, yx], ssem.at[12], planesem.at[y], (z, j, i, c))
+    row_of = lax.broadcasted_iota(jnp.int32, (8, 16), 0) + 2 * z
+    sel = (row_of == lax.broadcasted_iota(jnp.int32, (8, 16), 1)).astype(BF16)
+    hown[...] = jnp.concatenate([dot(sel, rows[q, yx])[0:2] for q in range(2)], axis=1).astype(BF16)
+    send(hown, hgot, ssem.at[22], rsem.at[21], partner)
 
     driven = step_wide * conv_inner
     first_row = lax.broadcasted_iota(jnp.int32, (8, 512), 0) == 0
@@ -319,30 +347,40 @@
         copies[i].wait()
 
     picked = None
+    gain_half = second_gain[:, own_span]
+    ones = jnp.ones((16, 1024), BF16)
     for d in (0, 1, 3, 2):
         j = y_at[d]
-        landed(rows.at[c, pl.ds(0, 3 if d == 0 else 4)], planesem.at[j], "rows_yx")
-        block = rows[c, pl.ds(pl.multiple_of(j * NX, NX), NX)].reshape(64, 1024)
+        landed(ww.at[pl.ds(0, 192 if d == 0 else 256)], planesem.at[j], "rows_yx")
+        four = pl.ds(pl.multiple_of(j * NX, NX), NX)
+        plain = jnp.concatenate(
+            [rows[q, four].reshape(64, 512) for q in range(2)], axis=1
+        ).astype(F32)
+        block = (plain * gain_half).astype(BF16)
         got = dot(pt[pl.ds(pl.multiple_of(j * 64, 64), 64)][:, 0:32], block, 0, 0)
         picked = got if picked is None else picked + got
         if d == 2:
             pickm[...] = picked.astype(BF16)
             send(pickm, pickp, ssem.at[13], rsem.at[13], partner)
-        pbuf[j] = dot(upl[...], block, 1, 1)
+        pbuf[j] = jnp.concatenate(
+            [dot(upl[...], block, 1, 1), dot(ones, (plain * plain).astype(BF16), 1, 1)], axis=0
+        )
     sums = jnp.concatenate([pbuf[j] for j in range(NY)], axis=1)
-    pmsg[...] = jnp.concatenate([sums[32:48], sums[16:32]], axis=0)
+    pmsg[...] = jnp.concatenate([sums[32:48], sums[16:24], sums[48:56]], axis=0)
     send(pmsg, pgot, ssem.at[18], rsem.at[18], partner)
     own16 = picked.astype(BF16)
     gate_pre = dot(own16, eg[own_span])
     up_pre = dot(own16, eu[own_span])
     landed(pgot, rsem.at[18], "pgot")
-    pre = sums[0:32] + pgot[...]
-    weight = sigmoid(jnp.sum(pre[16:19], axis=0, keepdims=True))
-    dact[...] = (silu(pre[0:16]).astype(BF16).astype(F32) * weight).astype(BF16)
+    pre = jnp.concatenate([sums[0:24], sums[48:56]], axis=0) + pgot[...]
+    scale = lax.rsqrt(pre[24:25] * (1.0 / 2048.0) + norm_eps)
+    slot_scale = jnp.sum(pk[...] * scale, axis=1, keepdims=True)
+    weight = sigmoid(jnp.sum(pre[16:19], axis=0, keepdims=True) * scale)
+    dact[...] = (silu(pre[0:16] * scale).astype(BF16).astype(F32) * weight).astype(BF16)
     send(dact, dactp, ssem.at[15], rsem.at[15], partner)
     landed(pickp, rsem.at[13], "pickp")
-    gate_pre = gate_pre + dot(pickp[...], eg[other_span])
-    up_pre = up_pre + dot(pickp[...], eu[other_span])
+    gate_pre = (gate_pre + dot(pickp[...], eg[other_span])) * slot_scale
+    up_pre = (up_pre + dot(pickp[...], eu[other_span])) * slot_scale
     glu_part = jnp.minimum(gate_pre, clamp_limit)
     lin_part = jnp.clip(up_pre, -clamp_limit, clamp_limit)
     activated = (glu_part * sigmoid(glu_alpha * glu_part) * (lin_part + 1.0)).astype(BF16)
@@ -396,27 +434,40 @@
         for i in range(1, NZ):
             total = total + frecv[2 * i + k].astype(F32)
         final += [total, narrow[k]]
-    result = hid[z].astype(F32) + jnp.concatenate(final, axis=1)
+    landed(hgot, rsem.at[21], "hgot")
+    own_half, other_half = hown[...].astype(F32), hgot[...].astype(F32)
+    hidden = jnp.concatenate(
+        [jnp.where(c == 0, own_half, other_half), jnp.where(c == 0, other_half, own_half)], axis=1
+    )
+    result = hidden + jnp.concatenate(final, axis=1)
     layer_out[...] = jnp.where(c == 0, result[0:1], result[1:2]).astype(BF16)
 
     for i, ref in enumerate((
         tok.at[pl.ds(0, NZY - 1)], wi.at[pl.ds(0, NX - 1)], wg.at[pl.ds(0, NX - 1)],
         rts.at[pl.ds(0, NZ - 1)], psend_i.at[pl.ds(0, NZY - 1)], psend_g.at[pl.ds(0, NZY - 1)],
         rts.at[pl.ds(0, 120)], None, ddp, precv_i.at[pl.ds(0, 15)],
-        orecv.at[pl.ds(0, 15)], tkz.at[pl.ds(0, NZ - 1)], rows.at[0, pl.ds(0, NYX - 1)],
+        None, tkz.at[pl.ds(0, NZ - 1)], ww.at[pl.ds(0, 960)],
         pickm, epart, dact, prs.at[pl.ds(0, NYX - 1)], frecv.at[pl.ds(0, 15)], pmsg, upp,
-        zrs.at[pl.ds(0, NZ - 1)], zrecv.at[pl.ds(0, 31)],
+        zrs.at[pl.ds(0, NZ - 1)], zrecv.at[pl.ds(0, 31)], hown,
     )):
         if ref is not None:
             landed(ref, ssem.at[i])
 
     @pl.when(keeper == c)
     def _():
-        landed(rows.at[0, pl.ds(0, NYX - 1)], ssem.at[7])
+        landed(ww.at[pl.ds(0, 960)], ssem.at[7])
 
     @pl.when(keeper != c)
     def _():
         landed(wo, ssem.at[7])
+
+    @pl.when(holder == c)
+    def _():
+        landed(orecv.at[pl.ds(0, NZ - 1)], ssem.at[10])
+
+    @pl.when(holder != c)
+    def _():
+        landed(orecv, ssem.at[10])
 
 
 def write_kernel(*refs):
@@ -467,18 +518,20 @@
             V((NZY, 2, 1024), BF16), V((NZY, 2, 1024), BF16),
             V((NZY, 2, 1024), BF16), V((NZY, 2, 1024), BF16),
             V((128, 2, 256), BF16), V((2, 8, 16, 1024), BF16), V((2, NZ, 2, 1024), BF16),
-            V((16, 128), BF16), V((2 * NZ, 16, 128), BF16), V((NZ, 2, 2048), BF16), V((NZ, 2, 2048), BF16),
-            V((2, NYX, 16, 1024), BF16), V((16, 1024), BF16), V((16, 256), BF16), V((16, 256), BF16),
+            V((16, 128), BF16), V((8, 16, 128), BF16), V((NZ, 2, 2048), BF16), V((2, 1024), BF16),
+            V((2, 1024), BF16),
+            V((2, NYX, 16, 512), BF16), V((16, 1024), BF16), V((16, 256), BF16), V((16, 256), BF16),
             V((32, 1024), BF16), V((32, 1024), BF16),
             V((NYX, 16, WIDE), BF16), V((NYX, 16, WIDE), BF16), V((NZ, 2, WIDE), BF16),
             V((2 * NZ, 2, WIDE), BF16), V((256, 128), BF16), V((48, 1024), BF16),
-            V((16, 1024), BF16), V((NY, 48, 64), F32), V((32, 256), F32), V((32, 256), F32),
+            V((16, 1024), BF16), V((NY, 64, 64), F32), V((32, 256), F32), V((32, 256), F32),
             V((32, 1024), BF16), V((32, 1024), BF16), V((NY, 64, WIDE), F32),
             V((256, 256), BF16), V((32, 256), BF16), V((NZ, 32, 1024 - WIDE), BF16),
             V((NZ, 32, 1024 - WIDE), BF16), V((NYX, 2, 1024 - WIDE), BF16),
-            V((2 * NYX, 2, 1024 - WIDE), BF16),
-            pltpu.SemaphoreType.DMA((8,)), pltpu.SemaphoreType.DMA((22,)),
-            pltpu.SemaphoreType.DMA((21,)), pltpu.SemaphoreType.DMA((NY,)),
+            V((2 * NYX, 2, 1024 - WIDE), BF16), V((32, 256), F32),
+            pltpu.SemaphoreType.DMA((8,)), pltpu.SemaphoreType.DMA((23,)),
+            pltpu.SemaphoreType.DMA((22,)), pltpu.SemaphoreType.DMA((NY,)),
+            pltpu.SemaphoreType.DMA((2,)),
         ],
         compiler_params=pltpu.CompilerParams(
             collective_id=0, has_side_effects=True, vmem_limit_bytes=56 * 1024 * 1024

time: 61.9 us -> 60.5 us (0.977)
  Pallas kernels: 61.1 us -> 59.7 us
    pallas_call x1, Pallas kernels: 60.1 us -> 58.7 us  [local(): pl.pallas_call(layer_kernel, out_shape=tuple((V(o.shape, o.dtype) for o i...]
where the time goes in v5:
time: 60.5 us; the launch traced here: 60.4 us
  Pallas kernels  59.7 us (99%)
  between operations  0.65 us (1%)
    pallas_call x1, Pallas kernels, local(): pl.pallas_call(layer_kernel, out_shape=tuple((V(o.shape, o.dtype) for o i...  58.7 us

profile of v5, /device:TPU:1, one launch (start us, length us, event | category | flops | bytes accessed | tf_op | source)
XLA Modules:
  0.0 60.4 jit_solution(5682041190874208409)
XLA Ops:
  0.6 58.7 %layer.1 = (bf16[1,2048]{1,0:T(2,128)(2,1)S(1)}, bf16[3,2,1024]{2,1,0:T(2,128)(2,1)S(1)}, bf16[2,3,2,256]{3,2,1,0:T(2,128)(2,1)S(1)}, f32[2,16,64,128]{3,2,1,0:T(8,128)S(1)}) custom-call(bf16[2,2048]{1,0:T(2,128)(2,1)} %refs_0_.1, f32[1,2048]{1,0:T(1,128)} %bitcast.16, bf16[16,2048]{1,0:T(8,128)(2,1)} %bitcast.12, bf16[3,2,1024]{2,1,0:T(2,128)(2,1)} %bitcast.15, ...), custom_call_target="tpu_custom_call" | custom-call | flops 2000000000 | bytes 16777216 | tf_op jit(solution)/shard_map/layer/pallas_call | solution.py:507
  59.3 1.0 %write.1 = (bf16[1,2048]{1,0:T(2,128)(2,1)}, bf16[3,2,1024]{2,1,0:T(2,128)(2,1)}, bf16[2,3,2,256]{3,2,1,0:T(2,128)(2,1)}, f32[2,16,64,128]{3,2,1,0:T(8,128)}) custom-call(bf16[1,2048]{1,0:T(2,128)(2,1)S(1)} %get-tuple-element.12.refs_0_, bf16[3,2,1024]{2,1,0:T(2,128)(2,1)S(1)} %get-tuple-element.13.refs_1_, ...), custom_call_target="tpu_custom_call" | custom-call | tf_op jit(solution)/shard_map/write/pallas_call | solution.py:543

commit v6 on v5

--- a/solution.py
+++ b/solution.py
@@ -19,6 +19,7 @@
 highest = lax.Precision.HIGHEST
 NZ, NY, NX = 8, 4, 4
 NZY, NYX = NZ * NY, NY * NX
+FAR = 12
 WIDE = 768
 
 
@@ -130,12 +131,13 @@
     with jax.named_scope("barrier"):
         pl.semaphore_wait(barrier, (NZY - 1) + (2 * NYX - 1) + (NZ - 1))
 
-    for k, j in zy_peers:
-        send(nblk.at[k * 2 + j // 2], tok.at[zy], ssem.at[0], rsem.at[0], (k, j, x, c))
+    for i in (x_at[2], x_at[1], x_at[3]):
+        send(wi.at[x], wi.at[x], ssem.at[1], rsem.at[1], (z, y, i, c))
+    for n, (k, j) in enumerate(zy_peers):
+        arrival = rsem.at[0] if n < FAR else rsem.at[22]
+        send(nblk.at[k * 2 + j // 2], tok.at[zy], ssem.at[0], arrival, (k, j, x, c))
     for k in z_peers:
         send(rts.at[base + z], rts.at[base + z], ssem.at[3], rsem.at[3], (k, y, x, c))
-    for i in (x_at[2], x_at[1], x_at[3]):
-        send(wi.at[x], wi.at[x], ssem.at[1], rsem.at[1], (z, y, i, c))
     for i in (x_at[2], x_at[1], x_at[3]):
         send(wg.at[x], wg.at[x], ssem.at[2], rsem.at[2], (z, y, i, c))
     for k in z_peers:
@@ -164,27 +166,49 @@
     read_proj = dot(normed, rw[...]).astype(BF16)
     step_raw = dot(normed, step_weight[...], 1, 1)
 
-    landed(tok.at[pl.ds(0, NZY - 1)], rsem.at[0], "tok")
+    low = (y % 2) == 0
+
+    def padded(weights):
+        weight = weights.reshape(64, 1024)[...]
+        zero = jnp.zeros_like(weight)
+        return jnp.concatenate([jnp.where(low, weight, zero), jnp.where(low, zero, weight)], axis=0)
+
+    def terms(lhs, rhs, out, places):
+        result = dot(lhs, rhs).astype(BF16)
+        for n, d in enumerate(places):
+            span = pl.ds(pl.multiple_of(z_at[d] * NY, NY), NY)
+            out[span] = result[8 * n : 8 * n + 8].reshape(NY, 2, 1024)
+
+    def tokens_of(places):
+        spans = [pl.ds(pl.multiple_of(z_at[d] * NY, NY), NY) for d in places]
+        return jnp.concatenate([tok[span].reshape(2 * NY, 128) for span in spans], axis=0)
+
+    def scatter(out, into, n, peers):
+        for k, j in peers:
+            send(out.at[k * NY + j], into.at[zy], ssem.at[n], rsem.at[n], (k, j, x, c))
+
+    near, far = (2, 6, 1, 7, 0), (4, 3, 5)
+    landed(wi.at[pl.ds(0, NX - 1)], rsem.at[1], "wi")
+    landed(tok.at[pl.ds(0, NZY - 1 - FAR)], rsem.at[22], "tok_near")
+    inner_rows = padded(wi)
+    near_tok = tokens_of(near)
+    terms(near_tok, inner_rows, psend_i, near)
+    scatter(psend_i, precv_i, 4, zy_peers[FAR:])
     landed(rts.at[pl.ds(0, NZ - 1)], rsem.at[3], "rt_z")
     mine8 = pl.ds(base, NZ)
     for j, i in yx_peers:
         send(rts.at[mine8], rts.at[mine8], ssem.at[6], rsem.at[6], (z, j, i, c))
-    landed(wi.at[pl.ds(0, NX - 1)], rsem.at[1], "wi")
-    all_tok = tok.reshape(2 * NZY, 128)[...]
-    low = (y % 2) == 0
-
-    def padded(weight):
-        zero = jnp.zeros_like(weight)
-        return jnp.concatenate([jnp.where(low, weight, zero), jnp.where(low, zero, weight)], axis=0)
-
-    psend_i.reshape(2 * NZY, 1024)[...] = dot(all_tok, padded(wi.reshape(64, 1024)[...])).astype(BF16)
-    for k, j in zy_peers:
-        send(psend_i.at[k * NY + j], precv_i.at[zy], ssem.at[4], rsem.at[4], (k, j, x, c))
+    landed(tok.at[pl.ds(0, FAR)], rsem.at[0], "tok")
+    far_tok = tokens_of(far)
+    terms(far_tok, inner_rows, psend_i, far)
+    scatter(psend_i, precv_i, 4, zy_peers[:FAR])
+    landed(wg.at[pl.ds(0, NX - 1)], rsem.at[2], "wg")
+    gate_rows = padded(wg)
+    terms(far_tok, gate_rows, psend_g, far)
+    scatter(psend_g, precv_g, 5, zy_peers[:FAR])
+    terms(near_tok, gate_rows, psend_g, near)
+    scatter(psend_g, precv_g, 5, zy_peers[FAR:])
     precv_i[zy] = psend_i[zy]
-    landed(wg.at[pl.ds(0, NX - 1)], rsem.at[2], "wg")
-    psend_g.reshape(2 * NZY, 1024)[...] = dot(all_tok, padded(wg.reshape(64, 1024)[...])).astype(BF16)
-    for k, j in zy_peers:
-        send(psend_g.at[k * NY + j], precv_g.at[zy], ssem.at[5], rsem.at[5], (k, j, x, c))
     precv_g[zy] = psend_g[zy]
     own_span = pl.ds(pl.multiple_of(c * 1024, 1024), 1024)
     other_span = pl.ds(pl.multiple_of(other * 1024, 1024), 1024)
@@ -371,16 +395,18 @@
     own16 = picked.astype(BF16)
     gate_pre = dot(own16, eg[own_span])
     up_pre = dot(own16, eu[own_span])
+    landed(pickp, rsem.at[13], "pickp")
     landed(pgot, rsem.at[18], "pgot")
+    gate_pre = gate_pre + dot(pickp[...], eg[other_span])
+    up_pre = up_pre + dot(pickp[...], eu[other_span])
     pre = jnp.concatenate([sums[0:24], sums[48:56]], axis=0) + pgot[...]
     scale = lax.rsqrt(pre[24:25] * (1.0 / 2048.0) + norm_eps)
     slot_scale = jnp.sum(pk[...] * scale, axis=1, keepdims=True)
     weight = sigmoid(jnp.sum(pre[16:19], axis=0, keepdims=True) * scale)
     dact[...] = (silu(pre[0:16] * scale).astype(BF16).astype(F32) * weight).astype(BF16)
     send(dact, dactp, ssem.at[15], rsem.at[15], partner)
-    landed(pickp, rsem.at[13], "pickp")
-    gate_pre = (gate_pre + dot(pickp[...], eg[other_span])) * slot_scale
-    up_pre = (up_pre + dot(pickp[...], eu[other_span])) * slot_scale
+    gate_pre = gate_pre * slot_scale
+    up_pre = up_pre * slot_scale
     glu_part = jnp.minimum(gate_pre, clamp_limit)
     lin_part = jnp.clip(up_pre, -clamp_limit, clamp_limit)
     activated = (glu_part * sigmoid(glu_alpha * glu_part) * (lin_part + 1.0)).astype(BF16)
@@ -396,14 +422,6 @@
     landed(epartp, rsem.at[14], "epart")
     both = (own_part + epartp[...].astype(F32)).astype(BF16)
 
-    first_z = dot(
-        jnp.concatenate([dense_turned, pz[...]], axis=0),
-        jnp.concatenate([down[:, WIDE:], both[:, WIDE:]], axis=0), 0, 0,
-    )
-    zsum[...] = first_z.astype(BF16).reshape(NZ, 32, 1024 - WIDE)
-    for k in z_peers:
-        send(zsum.at[k], zrs.at[z], ssem.at[20], rsem.at[16], (k, y, x, c))
-    zrs[z] = zsum[z]
     for d in (2, 1, 3, 0):
         j = y_at[d]
         span = pl.ds(pl.multiple_of(j * 64, 64), 64)
@@ -413,6 +431,14 @@
             i = x_at[e]
             send(tsum.at[j * NX + i], prs.at[yx], ssem.at[16], rsem.at[19], (z, j, i, c))
     prs[yx] = tsum[yx]
+    first_z = dot(
+        jnp.concatenate([dense_turned, pz[...]], axis=0),
+        jnp.concatenate([down[:, WIDE:], both[:, WIDE:]], axis=0), 0, 0,
+    )
+    zsum[...] = first_z.astype(BF16).reshape(NZ, 32, 1024 - WIDE)
+    for k in z_peers:
+        send(zsum.at[k], zrs.at[z], ssem.at[20], rsem.at[16], (k, y, x, c))
+    zrs[z] = zsum[z]
     landed(zrs.at[pl.ds(0, NZ - 1)], rsem.at[16], "sum_z1")
     zsend[...] = jnp.sum(zrs[...].astype(F32), axis=0).astype(BF16).reshape(NYX, 2, 1024 - WIDE)
     for j, i in yx_peers:
@@ -530,7 +556,7 @@
             V((NZ, 32, 1024 - WIDE), BF16), V((NYX, 2, 1024 - WIDE), BF16),
             V((2 * NYX, 2, 1024 - WIDE), BF16), V((32, 256), F32),
             pltpu.SemaphoreType.DMA((8,)), pltpu.SemaphoreType.DMA((23,)),
-            pltpu.SemaphoreType.DMA((22,)), pltpu.SemaphoreType.DMA((NY,)),
+            pltpu.SemaphoreType.DMA((23,)), pltpu.SemaphoreType.DMA((NY,)),
             pltpu.SemaphoreType.DMA((2,)),
         ],
         compiler_params=pltpu.CompilerParams(

time: 60.5 us -> 59.7 us (0.987)
  Pallas kernels: 59.7 us -> 58.9 us
    pallas_call x1, Pallas kernels: 58.7 us -> 57.9 us  [local(): pl.pallas_call(layer_kernel, out_shape=tuple((V(o.shape, o.dtype) for o i...]
where the time goes in v6:
time: 59.7 us; the launch traced here: 59.5 us
  Pallas kernels  58.9 us (99%)
  between operations  0.65 us (1%)
    pallas_call x1, Pallas kernels, local(): pl.pallas_call(layer_kernel, out_shape=tuple((V(o.shape, o.dtype) for o i...  57.9 us

profile of v6, /device:TPU:1, one launch (start us, length us, event | category | flops | bytes accessed | tf_op | source)
XLA Modules:
  0.0 59.5 jit_solution(1143852827868953042)
XLA Ops:
  0.6 57.9 %layer.1 = (bf16[1,2048]{1,0:T(2,128)(2,1)S(1)}, bf16[3,2,1024]{2,1,0:T(2,128)(2,1)S(1)}, bf16[2,3,2,256]{3,2,1,0:T(2,128)(2,1)S(1)}, f32[2,16,64,128]{3,2,1,0:T(8,128)S(1)}) custom-call(bf16[2,2048]{1,0:T(2,128)(2,1)} %refs_0_.1, f32[1,2048]{1,0:T(1,128)} %bitcast.16, bf16[16,2048]{1,0:T(8,128)(2,1)} %bitcast.12, bf16[3,2,1024]{2,1,0:T(2,128)(2,1)} %bitcast.15, ...), custom_call_target="tpu_custom_call" | custom-call | flops 2000000000 | bytes 16777216 | tf_op jit(solution)/shard_map/layer/pallas_call | solution.py:533
  58.5 1.0 %write.1 = (bf16[1,2048]{1,0:T(2,128)(2,1)}, bf16[3,2,1024]{2,1,0:T(2,128)(2,1)}, bf16[2,3,2,256]{3,2,1,0:T(2,128)(2,1)}, f32[2,16,64,128]{3,2,1,0:T(8,128)}) custom-call(bf16[1,2048]{1,0:T(2,128)(2,1)S(1)} %get-tuple-element.12.refs_0_, bf16[3,2,1024]{2,1,0:T(2,128)(2,1)S(1)} %get-tuple-element.13.refs_1_, ...), custom_call_target="tpu_custom_call" | custom-call | tf_op jit(solution)/shard_map/write/pallas_call | solution.py:569

commit v7 on v6

--- a/solution.py
+++ b/solution.py
@@ -349,7 +349,7 @@
         for i in range(4):
             rows[q, yx, :, i * 128 : (i + 1) * 128] = orecv[q * 4 + i]
         for j, i in yx_peers:
-            send(rows.at[q, yx], rows.at[q, yx], ssem.at[12], planesem.at[y], (z, j, i, c))
+            send(rows.at[q, yx], rows.at[q, yx], ssem.at[12], planesem.at[q * NY + y], (z, j, i, c))
     row_of = lax.broadcasted_iota(jnp.int32, (8, 16), 0) + 2 * z
     sel = (row_of == lax.broadcasted_iota(jnp.int32, (8, 16), 1)).astype(BF16)
     hown[...] = jnp.concatenate([dot(sel, rows[q, yx])[0:2] for q in range(2)], axis=1).astype(BF16)
@@ -370,35 +370,45 @@
     for i in (3, 4, 5):
         copies[i].wait()
 
-    picked = None
-    gain_half = second_gain[:, own_span]
-    ones = jnp.ones((16, 1024), BF16)
-    for d in (0, 1, 3, 2):
-        j = y_at[d]
-        landed(ww.at[pl.ds(0, 192 if d == 0 else 256)], planesem.at[j], "rows_yx")
-        four = pl.ds(pl.multiple_of(j * NX, NX), NX)
-        plain = jnp.concatenate(
-            [rows[q, four].reshape(64, 512) for q in range(2)], axis=1
-        ).astype(F32)
-        block = (plain * gain_half).astype(BF16)
-        got = dot(pt[pl.ds(pl.multiple_of(j * 64, 64), 64)][:, 0:32], block, 0, 0)
-        picked = got if picked is None else picked + got
-        if d == 2:
-            pickm[...] = picked.astype(BF16)
-            send(pickm, pickp, ssem.at[13], rsem.at[13], partner)
-        pbuf[j] = jnp.concatenate(
-            [dot(upl[...], block, 1, 1), dot(ones, (plain * plain).astype(BF16), 1, 1)], axis=0
-        )
+    ones = jnp.ones((16, 512), BF16)
+    own16 = []
+    for n in range(2):
+        q = near_group + n * (1 - 2 * near_group)
+        within = pl.ds(pl.multiple_of(q * 512, 512), 512)
+        span = pl.ds(pl.multiple_of(c * 1024 + q * 512, 512), 512)
+        gain_part = second_gain[:, span]
+        picked = None
+        for d in (2, 1, 3, 0):
+            j = y_at[d]
+            landed(ww.at[pl.ds(0, 96 if d == 0 else 128)], planesem.at[q * NY + j], "rows_yx")
+            plain = rows[q, pl.ds(pl.multiple_of(j * NX, NX), NX)].reshape(64, 512).astype(F32)
+            block = (plain * gain_part).astype(BF16)
+            got = dot(pt[pl.ds(pl.multiple_of(j * 64, 64), 64)][:, 0:32], block, 0, 0)
+            picked = got if picked is None else picked + got
+            if d == 0:
+                pickm[q] = picked.astype(BF16)
+                arrival = rsem.at[13 + 10 * n]
+                send(pickm.at[q], pickp.at[q], ssem.at[13 + 10 * n], arrival, partner)
+            both_sums = jnp.concatenate(
+                [dot(upl[:, within], block, 1, 1), dot(ones, (plain * plain).astype(BF16), 1, 1)],
+                axis=0,
+            )
+            pbuf[j] = both_sums if n == 0 else pbuf[j] + both_sums
+        own16.append(picked.astype(BF16))
+        if n == 0:
+            gate_pre = dot(own16[0], eg[span])
+            up_pre = dot(own16[0], eu[span])
     sums = jnp.concatenate([pbuf[j] for j in range(NY)], axis=1)
     pmsg[...] = jnp.concatenate([sums[32:48], sums[16:24], sums[48:56]], axis=0)
     send(pmsg, pgot, ssem.at[18], rsem.at[18], partner)
-    own16 = picked.astype(BF16)
-    gate_pre = dot(own16, eg[own_span])
-    up_pre = dot(own16, eu[own_span])
-    landed(pickp, rsem.at[13], "pickp")
+    gate_pre = gate_pre + dot(own16[1], eg[span])
+    up_pre = up_pre + dot(own16[1], eu[span])
+    landed(pickp.at[0], rsem.at[13], "pickp")
+    landed(pickp.at[0], rsem.at[23], "pickp2")
+    other16 = jnp.concatenate([pickp[0], pickp[1]], axis=1)
     landed(pgot, rsem.at[18], "pgot")
-    gate_pre = gate_pre + dot(pickp[...], eg[other_span])
-    up_pre = up_pre + dot(pickp[...], eu[other_span])
+    gate_pre = gate_pre + dot(other16, eg[other_span])
+    up_pre = up_pre + dot(other16, eu[other_span])
     pre = jnp.concatenate([sums[0:24], sums[48:56]], axis=0) + pgot[...]
     scale = lax.rsqrt(pre[24:25] * (1.0 / 2048.0) + norm_eps)
     slot_scale = jnp.sum(pk[...] * scale, axis=1, keepdims=True)
@@ -473,8 +483,9 @@
         rts.at[pl.ds(0, NZ - 1)], psend_i.at[pl.ds(0, NZY - 1)], psend_g.at[pl.ds(0, NZY - 1)],
         rts.at[pl.ds(0, 120)], None, ddp, precv_i.at[pl.ds(0, 15)],
         None, tkz.at[pl.ds(0, NZ - 1)], ww.at[pl.ds(0, 960)],
-        pickm, epart, dact, prs.at[pl.ds(0, NYX - 1)], frecv.at[pl.ds(0, 15)], pmsg, upp,
+        pickm.at[0], epart, dact, prs.at[pl.ds(0, NYX - 1)], frecv.at[pl.ds(0, 15)], pmsg, upp,
         zrs.at[pl.ds(0, NZ - 1)], zrecv.at[pl.ds(0, 31)], hown,
+        pickm.at[0],
     )):
         if ref is not None:
             landed(ref, ssem.at[i])
@@ -551,12 +562,12 @@
             V((NYX, 16, WIDE), BF16), V((NYX, 16, WIDE), BF16), V((NZ, 2, WIDE), BF16),
             V((2 * NZ, 2, WIDE), BF16), V((256, 128), BF16), V((48, 1024), BF16),
             V((16, 1024), BF16), V((NY, 64, 64), F32), V((32, 256), F32), V((32, 256), F32),
-            V((32, 1024), BF16), V((32, 1024), BF16), V((NY, 64, WIDE), F32),
+            V((2, 32, 512), BF16), V((2, 32, 512), BF16), V((NY, 64, WIDE), F32),
             V((256, 256), BF16), V((32, 256), BF16), V((NZ, 32, 1024 - WIDE), BF16),
             V((NZ, 32, 1024 - WIDE), BF16), V((NYX, 2, 1024 - WIDE), BF16),
             V((2 * NYX, 2, 1024 - WIDE), BF16), V((32, 256), F32),
-            pltpu.SemaphoreType.DMA((8,)), pltpu.SemaphoreType.DMA((23,)),
-            pltpu.SemaphoreType.DMA((23,)), pltpu.SemaphoreType.DMA((NY,)),
+            pltpu.SemaphoreType.DMA((8,)), pltpu.SemaphoreType.DMA((24,)),
+            pltpu.SemaphoreType.DMA((24,)), pltpu.SemaphoreType.DMA((2 * NY,)),
             pltpu.SemaphoreType.DMA((2,)),
         ],
         compiler_params=pltpu.CompilerParams(

time: 59.7 us -> 59.2 us (level)
  no operation moved by 1% of the time
where the time goes in v7:
time: 59.2 us; the launch traced here: 59 us
  Pallas kernels  58.4 us (99%)
  between operations  0.65 us (1%)
    pallas_call x1, Pallas kernels, local(): pl.pallas_call(layer_kernel, out_shape=tuple((V(o.shape, o.dtype) for o i...  57.4 us

profile of v7, /device:TPU:1, one launch (start us, length us, event | category | flops | bytes accessed | tf_op | source)
XLA Modules:
  0.0 59.0 jit_solution(109530090521947701)
XLA Ops:
  0.6 57.4 %layer.1 = (bf16[1,2048]{1,0:T(2,128)(2,1)S(1)}, bf16[3,2,1024]{2,1,0:T(2,128)(2,1)S(1)}, bf16[2,3,2,256]{3,2,1,0:T(2,128)(2,1)S(1)}, f32[2,16,64,128]{3,2,1,0:T(8,128)S(1)}) custom-call(bf16[2,2048]{1,0:T(2,128)(2,1)} %refs_0_.1, f32[1,2048]{1,0:T(1,128)} %bitcast.16, bf16[16,2048]{1,0:T(8,128)(2,1)} %bitcast.12, bf16[3,2,1024]{2,1,0:T(2,128)(2,1)} %bitcast.15, ...), custom_call_target="tpu_custom_call" | custom-call | flops 2000000000 | bytes 16777216 | tf_op jit(solution)/shard_map/layer/pallas_call | solution.py:544
  58.0 1.0 %write.1 = (bf16[1,2048]{1,0:T(2,128)(2,1)}, bf16[3,2,1024]{2,1,0:T(2,128)(2,1)}, bf16[2,3,2,256]{3,2,1,0:T(2,128)(2,1)}, f32[2,16,64,128]{3,2,1,0:T(8,128)}) custom-call(bf16[1,2048]{1,0:T(2,128)(2,1)S(1)} %get-tuple-element.12.refs_0_, bf16[3,2,1024]{2,1,0:T(2,128)(2,1)S(1)} %get-tuple-element.13.refs_1_, ...), custom_call_target="tpu_custom_call" | custom-call | tf_op jit(solution)/shard_map/write/pallas_call | solution.py:580
